TPU v7x, 32 devices: a whole 2x2x4 slice. The times are simulated.
32 devices in a mesh: ep: 8 (over z, y), tp: 4 (over x, core).
Axes of the slice: x: 2, y: 2, z: 4, core: 2. Of those that a mesh axis runs over, the one named last changes fastest.
Arguments:
- mixer_microbatch: bfloat16 [8192, 2048], P(('ep', 'tp')), may hold values from -6 to 6
- mixer_gain_vector: float32 [2048], replicated, may hold values from 0.1 to 1.9
- asker_matrix: bfloat16 [2048, 1024], P(None, 'tp'), may hold values from -0.125 to 0.125
- matcher_matrix: bfloat16 [2048, 1024], P(None, 'tp'), may hold values from -0.125 to 0.125
- fading_matrix: bfloat16 [2048, 1024], P(None, 'tp'), may hold values from -0.125 to 0.125
- content_matrix: bfloat16 [2048, 2048], P(None, 'tp'), may hold values from -0.125 to 0.125
- result_valve_matrix: bfloat16 [2048, 2048], P(None, 'tp'), may hold values from -0.125 to 0.125
- fading_shift_vector: float32 [1024], P('tp'), may hold values from -1.5 to 20
- extra_fade_amount: float32 [8192, 16], P('ep', 'tp'), may hold values from -0.7 to 0
- starting_memory: float32 [1024, 128], P('tp'), may hold values from -24 to 24
- subspace_gain_vector: float32 [2048], P('tp'), may hold values from 0.1 to 1.9
- result_matrix: bfloat16 [2048, 2048], replicated, may hold values from -0.125 to 0.125
- specialist_microbatch: bfloat16 [4096, 2048], P(('ep', 'tp')), may hold values from -6 to 6
- specialist_gain_vector: float32 [2048], replicated, may hold values from 0.1 to 1.9
- picked_specialists: int32 [4096, 2], P(('ep', 'tp')), may hold values from 0 to 15, all different within a row; in each aligned block of 128 rows (0 to 127, 128 to 255, ...) at most 24 rows name the same one
- specialist_mixing_factor: float32 [4096, 2], P(('ep', 'tp')), may hold values from 0.3 to 1.5
- specialist_valve_matrix: bfloat16 [16, 2048, 1024], P('ep', None, 'tp'), may hold values from -0.125 to 0.125
- specialist_widen_matrix: bfloat16 [16, 2048, 1024], P('ep', None, 'tp'), may hold values from -0.125 to 0.125
- specialist_shrink_matrix: bfloat16 [16, 1024, 2048], P('ep', 'tp'), may hold values from -0.1875 to 0.1875
- joint_valve_matrix: bfloat16 [2048, 512], P(None, 'tp'), may hold values from -0.125 to 0.125
- joint_widen_matrix: bfloat16 [2048, 512], P(None, 'tp'), may hold values from -0.125 to 0.125
- joint_shrink_matrix: bfloat16 [512, 2048], P('tp'), may hold values from -0.25 to 0.25
Outputs:
- mixer_sublayer_result: bfloat16 [8192, 2048], P(('ep', 'tp'))
- moe_out: bfloat16 [4096, 2048], P(('ep', 'tp'))
Inputs may be any that keep to these rules, and one draw needn't show every extreme that they name: `picked_specialists`: each row names 2 different experts; among the rows of one device no expert is named more than 24 times.
All inputs are finite; a program needn't handle non-finite values.
Results may differ from a plain program's by a relative error of at most 0.025.
Values may be sent and summed in bfloat16 or wider, within the bound.
No kernel may reach another device: no remote copies, remote signals or barrier semaphores. Data moves between devices by JAX's collectives and lax.ppermute only.
A program may use at most 192 MiB of HBM per device.

v0:
```python
import jax
import jax.numpy as jnp
from jax import lax
from jax.experimental import pallas as pl
from jax.experimental.pallas import tpu as pltpu
from jax.sharding import PartitionSpec as P

MATCHER_WIDTH = 64
DV = 128
SPAN_LENGTH = 64

NORM_EPS = 1e-06
GATE_SOFTNESS = 16.0
f32 = jnp.float32
bf16 = jnp.bfloat16


def params(**kw):
    return pltpu.CompilerParams(**kw)


def cost(flops, nbytes):
    return pl.CostEstimate(flops=int(flops), bytes_accessed=int(nbytes), transcendentals=0)


def vmem(count):
    return [pl.BlockSpec(memory_space=pltpu.VMEM)] * count


def dot(a, b, dims=((1,), (0,))):
    return lax.dot_general(a, b, (dims, ((), ())), preferred_element_type=f32)


def rms_rows(values, gain):
    widened = values.astype(f32)
    inverse_rms = lax.rsqrt(jnp.mean(widened * widened, axis=-1, keepdims=True) + NORM_EPS)
    return (widened * inverse_rms * gain).astype(bf16)


def silu(v):
    return v * jax.nn.sigmoid(v)


def split_two(v):
    high = v.astype(bf16)
    return high, (v - high.astype(f32)).astype(bf16)


def split_three(v):
    high = v.astype(bf16)
    rest = v - high.astype(f32)
    mid = rest.astype(bf16)
    return high, mid, (rest - mid.astype(f32)).astype(bf16)


def slot_choice(picks, factors, slot_expert, slot_place, experts):
    top, tokens = picks.shape
    slots = slot_expert.shape[0]
    index = lax.broadcasted_iota(jnp.int32, (experts, tokens), 0).astype(f32)
    named = jnp.zeros((experts, tokens), f32)
    weight = jnp.zeros((experts, tokens), f32)
    for k in range(top):
        hit = picks[k : k + 1, :] == index
        named = named + jnp.where(hit, 1.0, 0.0)
        weight = weight + jnp.where(hit, factors[k : k + 1, :], 0.0)
    row = lax.broadcasted_iota(jnp.int32, (tokens, tokens), 0)
    column = lax.broadcasted_iota(jnp.int32, (tokens, tokens), 1)
    earlier = jnp.where(row < column, 1.0, 0.0).astype(bf16)
    rank = dot(named.astype(bf16), earlier)
    spread = lax.broadcasted_iota(jnp.int32, (slots, experts), 1).astype(f32) == slot_expert
    spread = jnp.where(spread, 1.0, 0.0).astype(bf16)
    named_at = dot(spread, named.astype(bf16))
    rank_at = dot(spread, rank.astype(bf16))
    w1, w2, w3 = split_three(weight)
    weight_at = dot(spread, w1) + dot(spread, w2) + dot(spread, w3)
    chosen = (named_at > 0.5) & (rank_at == slot_place)
    return jnp.where(chosen, 1.0, 0.0).astype(bf16), jnp.where(chosen, weight_at, 0.0)


def pack_own_kernel(experts, slots, place_ref, x_ref, gain_ref, picks_ref, factor_ref, *refs):
    normed_ref, weight_ref = refs[:2]
    outs = refs[2:]
    normed = rms_rows(x_ref[...], gain_ref[...])
    normed_ref[...] = normed
    row = lax.broadcasted_iota(jnp.int32, (weight_ref.shape[0], 1), 0)
    block = jnp.zeros(row.shape, jnp.int32)
    for n in range(1, len(outs)):
        block = block + jnp.where(row >= n * slots, 1, 0)
    owner = jnp.bitwise_xor(block, place_ref[0])
    local = experts // len(outs)
    pick, weights = slot_choice(
        picks_ref[...].astype(f32),
        factor_ref[...],
        (owner * local).astype(f32),
        (row - block * slots).astype(f32),
        experts,
    )
    rows = dot(pick, normed).astype(bf16)
    for n, ref in enumerate(outs):
        ref[...] = rows[n * slots : (n + 1) * slots]
    weight_ref[...] = weights


def pack_both_kernel(
    experts,
    slots,
    groups,
    own_ref,
    x_ref,
    gain_ref,
    picks_ref,
    factor_ref,
    picks_x_ref,
    factor_x_ref,
    tok_ref,
    out_ref,
    weight_ref,
):
    tok_ref[...] = rms_rows(x_ref[...], gain_ref[...])
    row = lax.broadcasted_iota(jnp.int32, (weight_ref.shape[0], 1), 0)
    block = jnp.zeros(row.shape, jnp.int32)
    for n in range(1, groups):
        block = block + jnp.where(row >= n * slots, 1, 0)
    local = experts // groups
    tables = ((block * local + 1).astype(f32), (row - block * slots).astype(f32))
    own, weights = slot_choice(picks_ref[...].astype(f32), factor_ref[...], *tables, experts)
    other, _ = slot_choice(picks_x_ref[...].astype(f32), factor_x_ref[...], *tables, experts)
    weight_ref[...] = weights
    rows = (dot(own, own_ref[...]).astype(bf16), dot(other, tok_ref[...]).astype(bf16))
    for n in range(groups):
        for k in range(2):
            out_ref[(2 * n + k) * slots : (2 * n + k + 1) * slots] = rows[k][
                n * slots : (n + 1) * slots
            ]


def ffn_kernel(arrays, slots, *refs):
    ins = refs[:arrays]
    weights = refs[arrays : arrays + 6]
    outs = refs[arrays + 6 :]
    rows = jnp.concatenate([r[...] for r in ins], axis=0)
    total = None
    for n in range(2):
        gate_w, up_w, down_w = (w[...] for w in weights[3 * n : 3 * n + 3])
        if len(gate_w.shape) == 3:
            gate_w, up_w, down_w = gate_w[0], up_w[0], down_w[0]
        hidden = (silu(dot(rows, gate_w)) * dot(rows, up_w)).astype(bf16)
        part = dot(hidden, down_w)
        total = part if total is None else total + part
    height = ins[0].shape[0]
    if len(outs) == arrays:
        for k in range(arrays):
            outs[k][...] = total[k * height : (k + 1) * height].astype(bf16)
        return
    for n in range(height // (2 * slots)):
        for k in range(2):
            piece = total[(2 * n + k) * slots : (2 * n + k + 1) * slots].astype(bf16)
            outs[k][n * slots : (n + 1) * slots] = piece


def ffn(rows, weights, expert, steps, slots=None):
    arrays = len(rows)
    count, width = rows[0].shape
    height = count // steps
    row_spec = pl.BlockSpec((height, width), lambda i: (i, 0))
    if expert is None:
        weight_specs = [pl.BlockSpec(w.shape, lambda i: (0, 0)) for w in weights]
        inner = 2 * weights[0].shape[1]
    else:
        weight_specs = [
            pl.BlockSpec((1,) + w.shape[1:], lambda i: (expert, 0, 0)) for w in weights
        ]
        inner = 2 * weights[0].shape[2]
    if slots is None:
        outs, parts = arrays, 1
    else:
        outs, parts = 2, 2
    out = jax.ShapeDtypeStruct((count // parts, width), bf16)
    return pl.pallas_call(
        lambda *refs: ffn_kernel(arrays, slots, *refs),
        grid=(steps,),
        in_specs=[row_spec] * arrays + weight_specs,
        out_specs=[pl.BlockSpec((height // parts, width), lambda i: (i, 0))] * outs,
        out_shape=[out] * outs,
        compiler_params=params(),
        cost_estimate=cost(
            6 * arrays * count * width * inner, 4 * arrays * count * width + 6 * width * inner
        ),
    )(*rows, *weights)


def join_kernel(*refs):
    height = refs[0].shape[0]
    for n, ref in enumerate(refs[:-1]):
        refs[-1][n * height : (n + 1) * height, :] = ref[...]


def sum_kernel(a_ref, b_ref, *outs):
    total = (a_ref[...].astype(f32) + b_ref[...].astype(f32)).astype(bf16)
    height = outs[0].shape[0]
    for n, ref in enumerate(outs):
        ref[...] = total[n * height : (n + 1) * height]


def finish_kernel(near_weight_ref, far_weight_ref, shared_ref, got_ref, far_ref, *refs):
    out_ref = refs[-1]
    total = shared_ref[...].astype(f32) + got_ref[...].astype(f32)
    near = jnp.concatenate([r[...] for r in refs[:-1]], axis=0)
    for weight_ref, ret in ((near_weight_ref, near), (far_weight_ref, far_ref[...])):
        for part in split_two(weight_ref[...]):
            total = total + dot(part, ret, ((0,), (0,)))
    out_ref[...] = total.astype(bf16)


def column_split(kernel, ins, blocked, outs, steps, flops):
    specs = []
    for a, cut in zip(ins, blocked):
        lead = a.shape[:-1]
        zeros = (0,) * len(lead)
        if cut:
            specs.append(pl.BlockSpec(lead + (a.shape[-1] // steps,), lambda i, z=zeros: z + (i,)))
        else:
            specs.append(pl.BlockSpec(a.shape, lambda i, z=zeros: z + (0,)))
    out_specs = [
        pl.BlockSpec(o.shape[:-1] + (o.shape[-1] // steps,), lambda i: (0, i)) for o in outs
    ]
    return pl.pallas_call(
        kernel,
        grid=(steps,),
        in_specs=specs,
        out_specs=out_specs,
        out_shape=outs,
        compiler_params=params(),
        cost_estimate=cost(flops, sum(a.size * a.dtype.itemsize for a in ins)),
    )(*ins)


def local_kernel(heads, place_ref, first_ref, second_ref, *refs):
    (
        gain_ref,
        q_ref,
        k_ref,
        d_ref,
        v_ref,
        g_ref,
        shift_ref,
        fade_ref,
        out_ref,
        qg_ref,
        gate_ref,
        pack_ref,
        buffer,
        sems,
    ) = refs
    slot = pl.program_id(0)
    span = SPAN_LENGTH
    key_width = q_ref.shape[1]
    value_width = v_ref.shape[1]

    @pl.when(slot == 0)
    def _():
        for n, ref in enumerate((first_ref, second_ref)):
            pltpu.make_async_copy(ref, buffer.at[n], sems.at[n]).start()

    pltpu.make_async_copy(first_ref, buffer.at[slot], sems.at[slot]).wait()
    normed = rms_rows(buffer[slot], gain_ref[...])
    rows = normed.shape[0]
    query = dot(normed, q_ref[...]).astype(bf16).astype(f32) * MATCHER_WIDTH ** (-0.5)
    keys = dot(normed, k_ref[...]).astype(bf16).astype(f32)
    logits = dot(normed, d_ref[...]).astype(bf16).astype(f32) + shift_ref[...]
    value = dot(normed, v_ref[...]).astype(bf16)
    gate_ref[0] = dot(normed, g_ref[...]).astype(bf16)

    head_row = lax.broadcasted_iota(jnp.int32, (heads, key_width), 0)
    head_lane = lax.broadcasted_iota(jnp.int32, (heads, key_width), 1)
    low = head_row * MATCHER_WIDTH
    spread = jnp.where((head_lane >= low) & (head_lane < low + MATCHER_WIDTH), 1.0, 0.0).astype(bf16)
    f1, f2, f3 = split_three(fade_ref[...])
    fade = dot(f1, spread) + dot(f2, spread) + dot(f3, spread)
    soft = jnp.minimum(logits, 0.0) - jnp.log1p(jnp.exp(-jnp.abs(logits)))
    rate = soft / GATE_SOFTNESS + fade

    row = lax.broadcasted_iota(jnp.int32, (rows, rows), 0)
    column = lax.broadcasted_iota(jnp.int32, (rows, rows), 1)
    span_bits = span.bit_length() - 1
    same_span = jnp.right_shift(row, span_bits) == jnp.right_shift(column, span_bits)
    lower = jnp.where(same_span & (row >= column), 1.0, 0.0).astype(bf16)
    r1, r2, r3 = split_three(rate)
    running = dot(lower, r1) + dot(lower, r2) + dot(lower, r3)
    query_faded = query * jnp.exp(running)
    key_decayed = (keys * jnp.exp(-running)).astype(bf16)

    width_bits = MATCHER_WIDTH.bit_length() - 1
    value_bits = DV.bit_length() - 1
    lane_head = jnp.right_shift(
        lax.broadcasted_iota(jnp.int32, (span, key_width), 1), width_bits
    )
    causal = (
        jnp.bitwise_and(lax.broadcasted_iota(jnp.int32, (heads * span, span), 0), span - 1)
        >= lax.broadcasted_iota(jnp.int32, (heads * span, span), 1)
    )
    own_block = jnp.right_shift(
        lax.broadcasted_iota(jnp.int32, (value_width, key_width), 0), value_bits
    ) == jnp.right_shift(lax.broadcasted_iota(jnp.int32, (value_width, key_width), 1), width_bits)

    held = jnp.zeros((value_width, key_width), f32)
    passed = jnp.zeros((1, key_width), f32)
    for n in range(rows // span):
        at = slice(n * span, (n + 1) * span)
        qf = query_faded[at]
        total = running[(n + 1) * span - 1 : (n + 1) * span]
        qb = qf.astype(bf16)
        vb = value[at]
        key_end = (keys[at] * jnp.exp(total - running[at])).astype(bf16)
        stacked = jnp.concatenate(
            [jnp.where(lane_head == h, qf, 0.0) for h in range(heads)], axis=0
        ).astype(bf16)
        scores = dot(stacked, key_decayed[at], ((1,), (1,)))
        scores = jnp.where(causal, scores, 0.0).astype(bf16)
        inner = jnp.concatenate(
            [
                dot(scores[h * span : (h + 1) * span], vb[:, h * DV : (h + 1) * DV])
                for h in range(heads)
            ],
            axis=1,
        )
        outer = dot(qb, held.astype(bf16), ((1,), (1,)))
        out_ref[0, at, :] = inner + outer
        qg_ref[0, at, :] = (qf * jnp.exp(passed)).astype(bf16)
        added = dot(vb, key_end, ((0,), (0,)))
        held = held * jnp.exp(total) + jnp.where(own_block, added, 0.0)
        passed = passed + total
    compact = held[0:DV]
    for h in range(1, heads):
        compact = compact + held[h * DV : (h + 1) * DV]
    pack_ref[0, 0:DV, :] = compact
    pack_ref[0, DV:, :] = jnp.broadcast_to(
        jnp.exp(passed), (pack_ref.shape[1] - DV, key_width)
    )


def follow(held, pack):
    return held * pack[DV : DV + 1].astype(f32) + pack[0:DV].astype(f32)


def store_pack(ref, held, fading):
    ref[0:DV, :] = held.astype(bf16)
    ref[DV:, :] = jnp.broadcast_to(fading, (ref.shape[0] - DV, fading.shape[1])).astype(bf16)


def block_pack(packs, slot):
    inner = jnp.bitwise_and(slot, 1)
    return jnp.where(slot >= 2, packs[1][inner], packs[0][inner])


def chain_kernel(blocks, place_ref, first_ref, second_ref, out_ref):
    held = None
    for n in range(blocks):
        pack = block_pack((first_ref, second_ref), jnp.bitwise_xor(place_ref[1], n))
        if held is None:
            held, fading = pack[0:DV], pack[DV : DV + 1]
        else:
            held, fading = follow(held, pack), fading * pack[DV : DV + 1]
    store_pack(out_ref, held, fading)


def pair_kernel(place_ref, own_ref, got_ref, out_ref):
    own, got = own_ref[...].astype(f32), got_ref[...].astype(f32)
    odd = jnp.bitwise_and(place_ref[0], 1) == 1
    earlier, later = jnp.where(odd, got, own), jnp.where(odd, own, got)
    store_pack(
        out_ref, follow(earlier[0:DV], later), earlier[DV : DV + 1] * later[DV : DV + 1]
    )


def gated_kernel(
    heads,
    blocks,
    first_slot,
    place_ref,
    local_ref,
    qg_ref,
    gate_ref,
    gain_ref,
    start_ref,
    pack_a_ref,
    pack_b_ref,
    even_ref,
    *refs,
):
    outs = refs[-3:-1]
    packs = refs[:-3]
    entering = refs[-1]
    key_width = qg_ref.shape[2]

    @pl.when(pl.program_id(0) == 0)
    def _():
        held = start_ref[...]
        pair = jnp.right_shift(place_ref[0], 1)
        for shift in range(len(packs), 0, -1):
            held = jnp.where(pair >= shift, follow(held, packs[shift - 1][...]), held)
        odd = jnp.bitwise_and(place_ref[0], 1) == 1
        held = jnp.where(odd, follow(held, even_ref[...]), held)
        width_bits = MATCHER_WIDTH.bit_length() - 1
        lane_head = jnp.right_shift(
            lax.broadcasted_iota(jnp.int32, (DV, key_width), 1), width_bits
        )
        for n in range(blocks):
            slot = jnp.bitwise_xor(place_ref[1], n)
            for h in range(heads):
                entering[slot, h * DV : (h + 1) * DV, :] = jnp.where(
                    lane_head == h, held, 0.0
                ).astype(bf16)
            held = follow(held, block_pack((pack_a_ref, pack_b_ref), slot))

    slot = pl.program_id(0) + first_slot
    attended = local_ref[0] + dot(qg_ref[0], entering[slot], ((1,), (1,)))
    parts = []
    for h in range(heads):
        at = slice(h * DV, (h + 1) * DV)
        part = attended[:, at]
        inverse = lax.rsqrt(jnp.mean(part * part, axis=-1, keepdims=True) + NORM_EPS)
        part = part * inverse * gain_ref[:, at] * silu(gate_ref[0, :, at].astype(f32))
        parts.append(part.astype(bf16))
    rows = jnp.concatenate(parts, axis=1)
    for n, ref in enumerate(outs):

        @pl.when(pl.program_id(0) == n)
        def _(ref=ref):
            ref[...] = rows


def project_kernel(groups, place_ref, *refs):
    w_ref, out_ref = refs[groups:]
    width = refs[0].shape[1]
    total = None
    for n in range(groups):
        first = pl.multiple_of(jnp.bitwise_xor(place_ref[0], n) * width, width)
        part = dot(refs[n][...], w_ref[pl.ds(first, width), :])
        total = part if total is None else total + part
    out_ref[...] = total.astype(bf16)


def body(
    mixer_microbatch,
    mixer_gain_vector,
    asker_matrix,
    matcher_matrix,
    fading_matrix,
    content_matrix,
    result_valve_matrix,
    fading_shift_vector,
    extra_fade_amount,
    starting_memory,
    subspace_gain_vector,
    result_matrix,
    specialist_microbatch,
    specialist_gain_vector,
    picked_specialists,
    specialist_mixing_factor,
    specialist_valve_matrix,
    specialist_widen_matrix,
    specialist_shrink_matrix,
    joint_valve_matrix,
    joint_widen_matrix,
    joint_shrink_matrix,
):
    ep_count = lax.axis_size("ep")
    tp_count = lax.axis_size("tp")
    across = [(t, t ^ 2) for t in range(tp_count)]
    beside = [(t, t ^ 1) for t in range(tp_count)]
    ep_place = lax.axis_index("ep").astype(jnp.int32).reshape(1)
    tp_place = lax.axis_index("tp").astype(jnp.int32).reshape(1)

    tokens, feature_width = specialist_microbatch.shape
    top_count = picked_specialists.shape[1]
    local_experts = specialist_widen_matrix.shape[0]
    if local_experts != 2 or tp_count != 4:
        raise ValueError("unsupported sizes")
    experts = local_experts * ep_count
    slots = max(2, 3 * tokens * top_count // (2 * experts))

    picks, factors = picked_specialists.T, specialist_mixing_factor.T
    moe_raw_x = lax.ppermute(specialist_microbatch, "tp", across)
    picks_x = lax.ppermute(picks, "tp", across)
    factors_x = lax.ppermute(factors, "tp", across)
    mix_raw_x = lax.ppermute(mixer_microbatch, "tp", across)
    mix_raw_c = lax.ppermute(mixer_microbatch, "tp", beside)
    mix_raw_xc = lax.ppermute(mix_raw_x, "tp", beside)
    joint_weights = (joint_valve_matrix, joint_widen_matrix, joint_shrink_matrix)
    joint_weights += tuple(lax.ppermute(w, "tp", beside) for w in joint_weights)
    expert_weights = (specialist_valve_matrix, specialist_widen_matrix, specialist_shrink_matrix)
    expert_weights += tuple(lax.ppermute(w, "tp", beside) for w in expert_weights)

    near = ep_count * slots
    far = 2 * near
    moe_gain = specialist_gain_vector.reshape(1, -1)
    piece = jax.ShapeDtypeStruct((slots, feature_width), bf16)
    smem = [pl.BlockSpec(memory_space=pltpu.SMEM)]
    normed, near_weight, *near_out = pl.pallas_call(
        lambda *r: pack_own_kernel(experts, slots, *r),
        in_specs=smem + vmem(4),
        out_specs=vmem(2 + ep_count),
        out_shape=[
            jax.ShapeDtypeStruct((tokens, feature_width), bf16),
            jax.ShapeDtypeStruct((near, tokens), f32),
        ]
        + [piece] * ep_count,
        compiler_params=params(),
        cost_estimate=cost(2e9, 4e6),
        name="pack_own",
    )(ep_place, specialist_microbatch, moe_gain, picks, factors)

    def swap(pieces):
        return [pieces[0]] + [
            lax.ppermute(pieces[n], "ep", [(e, e ^ n) for e in range(ep_count)])
            for n in range(1, ep_count)
        ]

    def exchange(rows):
        shape = rows.shape
        cut = rows.reshape(ep_count, shape[0] // ep_count, shape[1])
        out = lax.all_to_all(cut, "ep", split_axis=0, concat_axis=0, tiled=True)
        return out.reshape(shape)

    near_in = pl.pallas_call(
        join_kernel,
        in_specs=vmem(ep_count),
        out_specs=pl.BlockSpec(memory_space=pltpu.VMEM),
        out_shape=jax.ShapeDtypeStruct((near, feature_width), bf16),
        compiler_params=params(),
        cost_estimate=cost(1e9, 2e6),
        name="near_join",
    )(*swap(near_out))

    normed_x, far_out, far_weight = pl.pallas_call(
        lambda *r: pack_both_kernel(experts, slots, ep_count, *r),
        in_specs=vmem(7),
        out_specs=vmem(3),
        out_shape=[
            jax.ShapeDtypeStruct((tokens, feature_width), bf16),
            jax.ShapeDtypeStruct((far, feature_width), bf16),
            jax.ShapeDtypeStruct((near, tokens), f32),
        ],
        compiler_params=params(),
        cost_estimate=cost(3e9, 6e6),
        name="pack_both",
    )(
        normed,
        moe_raw_x,
        moe_gain,
        picks,
        factors,
        picks_x,
        factors_x,
    )
    far_in = exchange(far_out)

    rows = mixer_microbatch.shape[0]
    key_width = asker_matrix.shape[1]
    value_width = content_matrix.shape[1]
    heads = value_width // DV
    pack_rows = DV + 16
    place = jnp.concatenate([ep_place, tp_place])
    whole = lambda a: pl.BlockSpec(a.shape, lambda i, *_: (0,) * len(a.shape))
    by_slot = lambda r, w: pl.BlockSpec((1, r, w), lambda i, *_: (i, 0, 0))
    mix_gain = mixer_gain_vector.reshape(1, -1)
    shift = fading_shift_vector.reshape(1, -1)
    weights = (asker_matrix, matcher_matrix, fading_matrix, content_matrix, result_valve_matrix)

    def local_part(raws, first_slot):
        fade_spec = pl.BlockSpec(
            (rows, heads), lambda i, p: (jnp.bitwise_xor(i + first_slot, p[1]), 0)
        )
        return pl.pallas_call(
            lambda *r: local_kernel(heads, *r),
            grid_spec=pltpu.PrefetchScalarGridSpec(
                num_scalar_prefetch=1,
                grid=(2,),
                in_specs=[pl.BlockSpec(memory_space=pl.ANY)] * 2
                + [whole(mix_gain)]
                + [whole(w) for w in weights]
                + [whole(shift), fade_spec],
                out_specs=[
                    by_slot(rows, value_width),
                    by_slot(rows, key_width),
                    by_slot(rows, value_width),
                    by_slot(pack_rows, key_width),
                ],
                scratch_shapes=[
                    pltpu.VMEM((2, rows, feature_width), bf16),
                    pltpu.SemaphoreType.DMA((2,)),
                ],
            ),
            out_shape=[
                jax.ShapeDtypeStruct((2, rows, value_width), f32),
                jax.ShapeDtypeStruct((2, rows, key_width), bf16),
                jax.ShapeDtypeStruct((2, rows, value_width), bf16),
                jax.ShapeDtypeStruct((2, pack_rows, key_width), f32),
            ],
            compiler_params=params(),
            cost_estimate=cost(1e10, 1e7),
        )(place, *raws, mix_gain, *weights, shift, extra_fade_amount)

    *part_a, pack_a = local_part((mixer_microbatch, mix_raw_c), 0)
    *part_b, pack_b = local_part((mix_raw_x, mix_raw_xc), 2)
    pack_shape = jax.ShapeDtypeStruct((pack_rows, key_width), bf16)

    def small_call(kernel, ins):
        return pl.pallas_call(
            kernel,
            in_specs=smem + vmem(len(ins)),
            out_specs=pl.BlockSpec(memory_space=pltpu.VMEM),
            out_shape=pack_shape,
            compiler_params=params(),
            cost_estimate=cost(1e9, 1e6),
        )(place, *ins)

    pack = small_call(lambda *r: chain_kernel(tp_count, *r), (pack_a, pack_b))
    got = lax.ppermute(pack, "ep", [(e, e ^ 1) for e in range(ep_count)])
    pair = small_call(pair_kernel, (pack, got))
    packs = [
        lax.ppermute(pair, "ep", [(e, e + 2 * s) for e in range(ep_count - 2 * s)])
        for s in range(1, ep_count // 2)
    ]
    start = starting_memory.T
    head_gain = subspace_gain_vector.reshape(1, -1)

    def gated_part(part, first_slot):
        ins = (head_gain, start, pack_a, pack_b, got, *packs)
        return pl.pallas_call(
            lambda *r: gated_kernel(heads, tp_count, first_slot, *r),
            grid_spec=pltpu.PrefetchScalarGridSpec(
                num_scalar_prefetch=1,
                grid=(2,),
                in_specs=[
                    by_slot(rows, value_width),
                    by_slot(rows, key_width),
                    by_slot(rows, value_width),
                ]
                + [whole(a) for a in ins],
                out_specs=[pl.BlockSpec((rows, value_width), lambda i, p: (0, 0))] * 2,
                scratch_shapes=[pltpu.VMEM((tp_count, value_width, key_width), bf16)],
            ),
            out_shape=[jax.ShapeDtypeStruct((rows, value_width), bf16)] * 2,
            compiler_params=params(),
            cost_estimate=cost(2e9, 6e6),
        )(place, *part, *ins)

    gated_b = gated_part(part_b, 2)
    gated_a = gated_part(part_a, 0)
    gated = [*gated_a, *gated_b]
    per_token = [gated[0]] + [
        lax.ppermute(gated[n], "tp", [(t, t ^ n) for t in range(tp_count)])
        for n in range(1, tp_count)
    ]

    near_x = lax.ppermute(near_in, "tp", across)
    shared_mine, shared_other = ffn([normed, normed_x], joint_weights, None, 1)
    shared_back = lax.ppermute(shared_other, "tp", across)
    near_mine, near_other = ffn([near_in, near_x], expert_weights, 0, 2)
    near_back = lax.ppermute(near_other, "tp", across)
    near_sum = pl.pallas_call(
        sum_kernel,
        in_specs=vmem(2),
        out_specs=vmem(ep_count),
        out_shape=[piece] * ep_count,
        compiler_params=params(),
        cost_estimate=cost(1e9, 3e6),
        name="near_sum",
    )(near_mine, near_back)
    near_ret = swap(near_sum)
    far_mine, far_other = ffn([far_in], expert_weights, 1, 2, slots)
    far_back = lax.ppermute(far_other, "tp", across)
    far_sum = pl.pallas_call(
        sum_kernel,
        in_specs=vmem(2),
        out_specs=pl.BlockSpec(memory_space=pltpu.VMEM),
        out_shape=jax.ShapeDtypeStruct((near, feature_width), bf16),
        compiler_params=params(),
        cost_estimate=cost(1e9, 3e6),
        name="far_sum",
    )(far_mine, far_back)
    far_ret = exchange(far_sum)
    (moe_out,) = column_split(
        finish_kernel,
        (near_weight, far_weight, shared_mine, shared_back, far_ret, *near_ret),
        (False, False, True, True, True) + (True,) * ep_count,
        [jax.ShapeDtypeStruct((tokens, feature_width), bf16)],
        2,
        8 * tokens * near * feature_width,
    )

    columns = 4
    out_width = result_matrix.shape[1]
    mixer_sublayer_result = pl.pallas_call(
        lambda *r: project_kernel(tp_count, *r),
        grid=(columns,),
        in_specs=smem
        + [pl.BlockSpec((rows, value_width), lambda i: (0, 0))] * tp_count
        + [
            pl.BlockSpec((result_matrix.shape[0], out_width // columns), lambda i: (0, i)),
        ],
        out_specs=pl.BlockSpec((rows, out_width // columns), lambda i: (0, i)),
        out_shape=jax.ShapeDtypeStruct((rows, out_width), bf16),
        compiler_params=params(),
        cost_estimate=cost(2 * rows * out_width * result_matrix.shape[0], 1e7),
        name="result_project",
    )(tp_place, *per_token, result_matrix)
    return (mixer_sublayer_result, moe_out)


def solution(mesh):
    return jax.shard_map(
        body,
        mesh=mesh,
        in_specs=(
            P(("ep", "tp"), None),
            P(),
            P(None, "tp"),
            P(None, "tp"),
            P(None, "tp"),
            P(None, "tp"),
            P(None, "tp"),
            P("tp"),
            P("ep", "tp"),
            P("tp", None),
            P("tp"),
            P(),
            P(("ep", "tp"), None),
            P(),
            P(("ep", "tp"), None),
            P(("ep", "tp"), None),
            P("ep", None, "tp"),
            P("ep", None, "tp"),
            P("ep", "tp", None),
            P(None, "tp"),
            P(None, "tp"),
            P("tp", None),
        ),
        out_specs=(P(("ep", "tp"), None), P(("ep", "tp"), None)),
        check_vma=False,
    )
```

profile of v0, /device:TPU:0, one launch (start us, length us, event | category | flops | bytes accessed | tf_op | source)
XLA Modules:
  0.0 217.8 jit_solution(1314570083166008245)
XLA Ops:
  0.6 3.0 %collective-permute-start.10 = (bf16[128,2048]{1,0:T(8,128)(2,1)}, bf16[128,2048]{1,0:T(8,128)(2,1)S(1)}, u32[]{:S(2)}, u32[]{:S(2)}) collective-permute-start(bf16[128,2048]{1,0:T(8,128)(2,1)} %r_1_.3), channel_id=1, source_target_pairs={{0,2},{1,3},{2,0},{3,1},{4,6},{5,7},{6,4},{7,5},{8,10},{9,11},{10,... | collective-permute-start | bytes 1572872 | tf_op jit(solution)/shard_map/ppermute | solution.py:484
  5.7 2.5 %pack_own.1 = (bf16[128,2048]{1,0:T(8,128)(2,1)}, f32[192,128]{1,0:T(8,128)}, bf16[24,2048]{1,0:T(8,128)(2,1)}, bf16[24,2048]{1,0:T(8,128)(2,1)}, bf16[24,2048]{...) custom-call(s32[1]{0:T(128)} %bitcast.1.r_0_, ...), custom_call_target="tpu_custom_call" | custom-call | flops 2000000000 | bytes 4000000 | tf_op jit(solution)/shard_map/pack_own/pallas_call | solution.py:500
  8.2 7.7 %collective-permute-done.11.r_5_ = s32[2,128]{1,0:T(2,128)S(1)} collective-permute-done((s32[2,128]{1,0:T(2,128)}, s32[2,128]{1,0:T(2,128)S(1)}, u32[]{:S(2)}, u32[]{:S(2)}) %collective-permute-start.11) | collective-permute-done | bytes 1056 | tf_op jit(solution)/shard_map/ppermute | solution.py:485
  16.7 3.3 %pack_both.1 = (bf16[128,2048]{1,0:T(8,128)(2,1)}, bf16[384,2048]{1,0:T(8,128)(2,1)}, f32[192,128]{1,0:T(8,128)}) custom-call(bf16[128,2048]{1,0:T(8,128)(2,1)} %get-tuple-element.54.r_0_.refs_0_, bf16[128,2048]{1,0:T(8,128)(2,1)} %copy-done.20, f32[1,2048]{1,0:T(1,128)} %bitcast.19, s32[2,128]{1,0:T(2,128)} %bitcast.26, f32[2,128]{1,0:T(2,128)} %bitcast.29, ...), custom_call_target="tpu_custom_call" | custom-call | flops 3000000000 | bytes 6000000 | tf_op jit(solution)/shard_map/pack_both/pallas_call | solution.py:536
  20.1 6.2 %all-to-all-start = ((bf16[8,48,2048]{2,1,0:T(8,128)(2,1)}), bf16[8,48,2048]{2,1,0:T(8,128)(2,1)}, u32[]{:S(2)}, u32[]{:S(2)}) async-start(bf16[8,48,2048]{2,1,0:T(8,128)(2,1)} %bitcast.14), calls=%async_computation | async-start | bytes 3145728 | tf_op jit(solution)/shard_map/all_to_all | solution.py:523
  30.4 10.9 %collective-permute-done.21.refs_1_ = bf16[24,2048]{1,0:T(8,128)(2,1)S(1)} collective-permute-done((bf16[24,2048]{1,0:T(8,128)(2,1)S(1)}, bf16[24,2048]{1,0:T(8,128)(2,1)S(1)}, u32[]{:S(2)}, u32[]{:S(2)}) %collective-permute-start.21) | collective-permute-done | bytes 98336 | tf_op jit(solution)/shard_map/ppermute | solution.py:516
  41.3 2.7 %collective-permute-start.23 = (bf16[24,2048]{1,0:T(8,128)(2,1)S(1)}, bf16[24,2048]{1,0:T(8,128)(2,1)S(1)}, u32[]{:S(2)}, u32[]{:S(2)}) collective-permute-start(bf16[24,2048]{1,0:T(8,128)(2,1)S(1)} %copy-done.27), channel_id=1, source_target_pairs={{0,12},{4,8},{8,4},{12,0},{16,28},{20,24},{24,20},{28,16},{1,13},{... | collective-permute-start | bytes 294920 | tf_op jit(solution)/shard_map/ppermute | solution.py:516
  44.0 10.1 %collective-permute-done.22.refs_2_ = bf16[24,2048]{1,0:T(8,128)(2,1)S(1)} collective-permute-done((bf16[24,2048]{1,0:T(8,128)(2,1)S(1)}, bf16[24,2048]{1,0:T(8,128)(2,1)S(1)}, u32[]{:S(2)}, u32[]{:S(2)}) %collective-permute-start.22) | collective-permute-done | bytes 98336 | tf_op jit(solution)/shard_map/ppermute | solution.py:516
  54.1 5.6 %collective-permute-start.24 = (bf16[24,2048]{1,0:T(8,128)(2,1)S(1)}, bf16[24,2048]{1,0:T(8,128)(2,1)S(1)}, u32[]{:S(2)}, u32[]{:S(2)}) collective-permute-start(bf16[24,2048]{1,0:T(8,128)(2,1)S(1)} %copy-done.24), channel_id=1, source_target_pairs={{0,16},{4,20},{8,24},{12,28},{16,0},{20,4},{24,8},{28,12},{1,17},{... | collective-permute-start | bytes 294920 | tf_op jit(solution)/shard_map/ppermute | solution.py:516
  59.7 2.5 %collective-permute-start.25 = (bf16[24,2048]{1,0:T(8,128)(2,1)S(1)}, bf16[24,2048]{1,0:T(8,128)(2,1)S(1)}, u32[]{:S(2)}, u32[]{:S(2)}) collective-permute-start(bf16[24,2048]{1,0:T(8,128)(2,1)S(1)} %copy-done.23), channel_id=1, source_target_pairs={{0,20},{4,16},{8,28},{12,24},{16,4},{20,0},{24,12},{28,8},{1,21},{... | collective-permute-start | bytes 294920 | tf_op jit(solution)/shard_map/ppermute | solution.py:516
  62.2 7.6 %collective-permute-done.24.refs_4_ = bf16[24,2048]{1,0:T(8,128)(2,1)S(1)} collective-permute-done((bf16[24,2048]{1,0:T(8,128)(2,1)S(1)}, bf16[24,2048]{1,0:T(8,128)(2,1)S(1)}, u32[]{:S(2)}, u32[]{:S(2)}) %collective-permute-start.24) | collective-permute-done | bytes 98336 | tf_op jit(solution)/shard_map/ppermute | solution.py:516
  73.5 4.7 %collective-permute-done.26.refs_6_ = bf16[24,2048]{1,0:T(8,128)(2,1)S(1)} collective-permute-done((bf16[24,2048]{1,0:T(8,128)(2,1)S(1)}, bf16[24,2048]{1,0:T(8,128)(2,1)S(1)}, u32[]{:S(2)}, u32[]{:S(2)}) %collective-permute-start.26) | collective-permute-done | bytes 98336 | tf_op jit(solution)/shard_map/ppermute | solution.py:516
  79.4 6.1 %collective-permute-done.27.refs_7_ = bf16[24,2048]{1,0:T(8,128)(2,1)S(1)} collective-permute-done((bf16[24,2048]{1,0:T(8,128)(2,1)S(1)}, bf16[24,2048]{1,0:T(8,128)(2,1)S(1)}, u32[]{:S(2)}, u32[]{:S(2)}) %collective-permute-start.27) | collective-permute-done | bytes 98336 | tf_op jit(solution)/shard_map/ppermute | solution.py:516
  94.2 7.0 %shard_map.228 = (bf16[192,2048]{1,0:T(8,128)(2,1)}, bf16[192,2048]{1,0:T(8,128)(2,1)}) custom-call(bf16[384,2048]{1,0:T(8,128)(2,1)} %bitcast.10.refs_0_, bf16[2,2048,256]{2,1,0:T(8,128)(2,1)} %refs_2_.5, bf16[2,2048,256]{2,1,0:T(8,128)(2,1)} %refs_3_.5, bf16[2,256,2048]{2,1,0:T(8,128)(2,1)} %refs_4_.3, ...), custom_call_target="tpu_custom_call" | custom-call | flops 2415919104 | bytes 9437184 | tf_op jit(solution)/shard_map/pallas_call | solution.py:179
  101.9 13.8 %shard_map.221 = (f32[2,256,512]{2,1,0:T(8,128)}, bf16[2,256,256]{2,1,0:T(8,128)(2,1)}, bf16[2,256,512]{2,1,0:T(8,128)(2,1)}, f32[2,144,256]{2,1,0:T(8,128)}) custom-call(s32[2]{0:T(128)} %pad_add_fusion.r_0_.place_ref, bf16[256,2048]{1,0:T(8,128)(2,1)} %r_1_.2, bf16[256,2048]{1,0:T(8,128)(2,1)} %collective-permute-done.r_2_, f32[1,2048]{1,0:T(1,128)} %bitcast.20, ...), custom_call_target="tpu_custom_call" | custom-call | flops 10000000000 | bytes 10000000 | tf_op jit(solution)/shard_map/pallas_call | solution.py:575
  116.7 7.0 %shard_map.229 = (bf16[192,2048]{1,0:T(8,128)(2,1)}, bf16[192,2048]{1,0:T(8,128)(2,1)}) custom-call(bf16[192,2048]{1,0:T(8,128)(2,1)} %near_join.1.refs_0_, bf16[192,2048]{1,0:T(8,128)(2,1)} %copy-done.2, bf16[2,2048,256]{2,1,0:T(8,128)(2,1)} %refs_2_.5, bf16[2,2048,256]{2,1,0:T(8,128)(2,1)} %refs_3_.5, bf16[2,256,2048]{2,1,0:T(8,128)(2,1)} %refs_4_.3, ...), custom_call_target="tpu_custom_call" | custom-call | flops 2415919104 | bytes 9437184 | tf_op jit(solution)/shard_map/pallas_call | solution.py:179
  123.7 5.7 %collective-permute-done.20.b_ref = bf16[192,2048]{1,0:T(8,128)(2,1)} collective-permute-done((bf16[192,2048]{1,0:T(8,128)(2,1)}, bf16[192,2048]{1,0:T(8,128)(2,1)}, u32[]{:S(2)}, u32[]{:S(2)}) %collective-permute-start.20) | collective-permute-done | bytes 786464 | tf_op jit(solution)/shard_map/ppermute | solution.py:674
  130.9 2.4 %far_sum.1 = bf16[192,2048]{1,0:T(8,128)(2,1)} custom-call(bf16[192,2048]{1,0:T(8,128)(2,1)} %get-tuple-element.60.a_ref, bf16[192,2048]{1,0:T(8,128)(2,1)} %collective-permute-done.20.b_ref), custom_call_target="tpu_custom_call" | custom-call | flops 1000000000 | bytes 3000000 | tf_op jit(solution)/shard_map/far_sum/pallas_call | solution.py:675
  133.3 5.8 %all-to-all-start.1 = ((bf16[8,24,2048]{2,1,0:T(8,128)(2,1)}), bf16[8,24,2048]{2,1,0:T(8,128)(2,1)S(1)}, u32[]{:S(2)}, u32[]{:S(2)}) async-start(bf16[8,24,2048]{2,1,0:T(8,128)(2,1)} %bitcast.15), calls=%async_computation.1 | async-start | bytes 1572864 | tf_op jit(solution)/shard_map/all_to_all | solution.py:523
  139.2 13.8 %shard_map.222 = (f32[2,256,512]{2,1,0:T(8,128)}, bf16[2,256,256]{2,1,0:T(8,128)(2,1)}, bf16[2,256,512]{2,1,0:T(8,128)(2,1)}, f32[2,144,256]{2,1,0:T(8,128)}) custom-call(s32[2]{0:T(128)} %pad_add_fusion.r_0_.place_ref, bf16[256,2048]{1,0:T(8,128)(2,1)} %collective-permute-done.1.r_1_, bf16[256,2048]{1,0:T(8,128)(2,1)} %collective-permute-done.2.r_2_, ...), custom_call_target="tpu_custom_call" | custom-call | flops 10000000000 | bytes 10000000 | tf_op jit(solution)/shard_map/pallas_call | solution.py:575
  161.5 3.9 %collective-permute-start.4 = (bf16[144,256]{1,0:T(8,128)(2,1)}, bf16[144,256]{1,0:T(8,128)(2,1)S(1)}, u32[]{:S(2)}, u32[]{:S(2)}) collective-permute-start(bf16[144,256]{1,0:T(8,128)(2,1)} %shard_map.224), channel_id=1, source_target_pairs={{0,8},{4,12},{8,16},{12,20},{16,24},{20,28},{1,9},{5,13},{9,17},{1... | collective-permute-start | bytes 221192 | tf_op jit(solution)/shard_map/ppermute | solution.py:623
  165.4 4.3 %collective-permute-start.5 = (bf16[144,256]{1,0:T(8,128)(2,1)}, bf16[144,256]{1,0:T(8,128)(2,1)S(1)}, u32[]{:S(2)}, u32[]{:S(2)}) collective-permute-start(bf16[144,256]{1,0:T(8,128)(2,1)} %shard_map.224), channel_id=1, source_target_pairs={{0,16},{4,20},{8,24},{12,28},{1,17},{5,21},{9,25},{13,29},{2,18},{... | collective-permute-start | bytes 221192 | tf_op jit(solution)/shard_map/ppermute | solution.py:623
  171.1 5.0 %shard_map.227 = (bf16[128,2048]{1,0:T(8,128)(2,1)}, bf16[128,2048]{1,0:T(8,128)(2,1)}) custom-call(bf16[128,2048]{1,0:T(8,128)(2,1)} %get-tuple-element.54.r_0_.refs_0_, bf16[128,2048]{1,0:T(8,128)(2,1)} %get-tuple-element.56.refs_1_, bf16[2048,128]{1,0:T(8,128)(2,1)} %refs_2_.3, bf16[2048,128]{1,0:T(8,128)(2,1)} %refs_3_.3, bf16[128,2048]{1,0:T(8,128)(2,1)} %refs_4_.2, ...), custom_call_target="tpu_custom_call" | custom-call | flops 805306368 | bytes 5242880 | tf_op jit(solution)/shard_map/pallas_call | solution.py:179
  177.3 4.3 %shard_map.226 = (bf16[256,512]{1,0:T(8,128)(2,1)}, bf16[256,512]{1,0:T(8,128)(2,1)}) custom-call(s32[2]{0:T(128)} %pad_add_fusion.r_0_.place_ref, f32[2,256,512]{2,1,0:T(8,128)} %get-tuple-element.48.r_1_, bf16[2,256,256]{2,1,0:T(8,128)(2,1)} %get-tuple-element.49.r_2_, bf16[2,256,512]{2,1,0:T(8,128)(2,1)} %get-tuple-element.50.r_3_, f32[1,512]{1,0:T(1,128)} %bitcast.22, ...), custom_call_target="tpu_custom_call" | custom-call | flops 2000000000 | bytes 6000000 | tf_op jit(solution)/shard_map/pallas_call | solution.py:631
  183.1 4.3 %shard_map.225 = (bf16[256,512]{1,0:T(8,128)(2,1)}, bf16[256,512]{1,0:T(8,128)(2,1)}) custom-call(s32[2]{0:T(128)} %pad_add_fusion.r_0_.place_ref, f32[2,256,512]{2,1,0:T(8,128)} %get-tuple-element.41.r_1_, bf16[2,256,256]{2,1,0:T(8,128)(2,1)} %get-tuple-element.42.r_2_, bf16[2,256,512]{2,1,0:T(8,128)(2,1)} %get-tuple-element.43.r_3_, f32[1,512]{1,0:T(1,128)} %bitcast.23, ...), custom_call_target="tpu_custom_call" | custom-call | flops 2000000000 | bytes 6000000 | tf_op jit(solution)/shard_map/pallas_call | solution.py:631
  188.0 2.3 %near_sum.1 = (bf16[24,2048]{1,0:T(8,128)(2,1)}, bf16[24,2048]{1,0:T(8,128)(2,1)}, bf16[24,2048]{1,0:T(8,128)(2,1)}, bf16[24,2048]{1,0:T(8,128)(2,1)}, bf16[24,2...) custom-call(bf16[192,2048]{1,0:T(8,128)(2,1)} %get-tuple-element.70.a_ref, ...), custom_call_target="tpu_custom_call" | custom-call | flops 1000000000 | bytes 3000000 | tf_op jit(solution)/shard_map/near_sum/pallas_call | solution.py:663
  191.7 3.5 %collective-permute-done.8.r_3_ = bf16[256,512]{1,0:T(8,128)(2,1)S(1)} collective-permute-done((bf16[256,512]{1,0:T(8,128)(2,1)}, bf16[256,512]{1,0:T(8,128)(2,1)S(1)}, u32[]{:S(2)}, u32[]{:S(2)}) %collective-permute-start.8) | collective-permute-done | bytes 262176 | tf_op jit(solution)/shard_map/ppermute | solution.py:654
  196.2 3.8 %collective-permute-start.34 = (bf16[24,2048]{1,0:T(8,128)(2,1)}, bf16[24,2048]{1,0:T(8,128)(2,1)S(1)}, u32[]{:S(2)}, u32[]{:S(2)}) collective-permute-start(bf16[24,2048]{1,0:T(8,128)(2,1)} %get-tuple-element.77), channel_id=1, source_target_pairs={{0,20},{4,16},{8,28},{12,24},{16,4},{20,0},{24,12},{28,8},{1,21},{... | collective-permute-start | bytes 294920 | tf_op jit(solution)/shard_map/ppermute | solution.py:516
  200.6 3.3 %collective-permute-start.36 = (bf16[24,2048]{1,0:T(8,128)(2,1)}, bf16[24,2048]{1,0:T(8,128)(2,1)S(1)}, u32[]{:S(2)}, u32[]{:S(2)}) collective-permute-start(bf16[24,2048]{1,0:T(8,128)(2,1)} %get-tuple-element.79), channel_id=1, source_target_pairs={{0,28},{4,24},{8,20},{12,16},{16,12},{20,8},{24,4},{28,0},{1,29},{... | collective-permute-start | bytes 294920 | tf_op jit(solution)/shard_map/ppermute | solution.py:516
  203.9 6.6 %result_project.1 = bf16[256,2048]{1,0:T(8,128)(2,1)} custom-call(s32[1]{0:T(128)} %bitcast.r_0_, bf16[256,512]{1,0:T(8,128)(2,1)} %get-tuple-element.46.r_1_, bf16[256,512]{1,0:T(8,128)(2,1)} %copy-done.10, bf16[256,512]{1,0:T(8,128)(2,1)} %copy-done.8, bf16[256,512]{1,0:T(8,128)(2,1)} %copy-done.9, bf16[2048,2048]{1,0:T(8,128)(2,1)} %r_5_.5), custom_call_target="tpu_custom_call" | custom-call | flops 2147483648 | bytes 10000000 | tf_op jit(solution)/shard_map/result_project/pallas_call | solution.py:696
  210.9 2.7 %collective-permute-done.34.refs_5_ = bf16[24,2048]{1,0:T(8,128)(2,1)S(1)} collective-permute-done((bf16[24,2048]{1,0:T(8,128)(2,1)}, bf16[24,2048]{1,0:T(8,128)(2,1)S(1)}, u32[]{:S(2)}, u32[]{:S(2)}) %collective-permute-start.34) | collective-permute-done | bytes 98336 | tf_op jit(solution)/shard_map/ppermute | solution.py:516
  214.6 3.2 %shard_map.230 = bf16[128,2048]{1,0:T(8,128)(2,1)} custom-call(f32[192,128]{1,0:T(8,128)} %get-tuple-element.53.near_weight_ref, f32[192,128]{1,0:T(8,128)} %get-tuple-element.55.far_weight_ref, bf16[128,2048]{1,0:T(8,128)(2,1)} %get-tuple-element.57.shared_ref, bf16[128,2048]{1,0:T(8,128)(2,1)} %copy-done.3, bf16[192,2048]{1,0:T(8,128)(2,1)} %bitcast.13, ...), custom_call_target="tpu_custom_call" | custom-call | flops 402653184 | bytes 2818048 | tf_op jit(solution)/shard_map/pallas_call | solution.py:227
  (147 shorter events, 41.1 us)
Async XLA Ops:
  0.6 15.3 %collective-permute-start.10 = (bf16[128,2048]{1,0:T(8,128)(2,1)}, bf16[128,2048]{1,0:T(8,128)(2,1)S(1)}, u32[]{:S(2)}, u32[]{:S(2)}) collective-permute-start(bf16[128,2048]{1,0:T(8,128)(2,1)} %r_1_.3), channel_id=1, source_target_pairs={{0,2},{1,3},{2,0},{3,1},{4,6},{5,7},{6,4},{7,5},{8,10},{9,11},{10,... | collective-permute-start | bytes 1572872 | tf_op jit(solution)/shard_map/ppermute | solution.py:484
  3.7 12.2 %collective-permute-start.11 = (s32[2,128]{1,0:T(2,128)}, s32[2,128]{1,0:T(2,128)S(1)}, u32[]{:S(2)}, u32[]{:S(2)}) collective-permute-start(s32[2,128]{1,0:T(2,128)} %bitcast.24), channel_id=1, source_target_pairs={{0,2},{1,3},{2,0},{3,1},{4,6},{5,7},{6,4},{7,5},{8,10},{9,11},{10,... | collective-permute-start | bytes 3080 | tf_op jit(solution)/shard_map/ppermute | solution.py:485
  3.7 12.1 %collective-permute-start.12 = (f32[2,128]{1,0:T(2,128)}, f32[2,128]{1,0:T(2,128)S(1)}, u32[]{:S(2)}, u32[]{:S(2)}) collective-permute-start(f32[2,128]{1,0:T(2,128)} %bitcast.27), channel_id=1, source_target_pairs={{0,2},{1,3},{2,0},{3,1},{4,6},{5,7},{6,4},{7,5},{8,10},{9,11},{10,... | collective-permute-start | bytes 3080 | tf_op jit(solution)/shard_map/ppermute | solution.py:486
  20.1 74.1 %all-to-all-start = ((bf16[8,48,2048]{2,1,0:T(8,128)(2,1)}), bf16[8,48,2048]{2,1,0:T(8,128)(2,1)}, u32[]{:S(2)}, u32[]{:S(2)}) async-start(bf16[8,48,2048]{2,1,0:T(8,128)(2,1)} %bitcast.14), calls=%async_computation | async-start | bytes 3145728 | tf_op jit(solution)/shard_map/all_to_all | solution.py:523
  26.3 65.9 %collective-permute-start.17 = (bf16[2,2048,256]{2,1,0:T(8,128)(2,1)S(1)}, bf16[2,2048,256]{2,1,0:T(8,128)(2,1)}, u32[]{:S(2)}, u32[]{:S(2)}) collective-permute-start(bf16[2,2048,256]{2,1,0:T(8,128)(2,1)S(1)} %copy-done), channel_id=1, source_target_pairs={{0,1},{1,0},{2,3},{3,2},{4,5},{5,4},{6,7},{7,6},{8,9},{9,8},{10,11... | collective-permute-start | bytes 6291464 | tf_op jit(solution)/shard_map/ppermute | solution.py:493
  26.4 66.3 %collective-permute-start.18 = (bf16[2,2048,256]{2,1,0:T(8,128)(2,1)}, bf16[2,2048,256]{2,1,0:T(8,128)(2,1)}, u32[]{:S(2)}, u32[]{:S(2)}) collective-permute-start(bf16[2,2048,256]{2,1,0:T(8,128)(2,1)} %refs_3_.5), channel_id=1, source_target_pairs={{0,1},{1,0},{2,3},{3,2},{4,5},{5,4},{6,7},{7,6},{8,9},{9,8},{10,11... | collective-permute-start | bytes 6291464 | tf_op jit(solution)/shard_map/ppermute | solution.py:493
  26.9 67.3 %collective-permute-start.19 = (bf16[2,256,2048]{2,1,0:T(8,128)(2,1)}, bf16[2,256,2048]{2,1,0:T(8,128)(2,1)}, u32[]{:S(2)}, u32[]{:S(2)}) collective-permute-start(bf16[2,256,2048]{2,1,0:T(8,128)(2,1)} %refs_4_.3), channel_id=1, source_target_pairs={{0,1},{1,0},{2,3},{3,2},{4,5},{5,4},{6,7},{7,6},{8,9},{9,8},{10,11... | collective-permute-start | bytes 6291464 | tf_op jit(solution)/shard_map/ppermute | solution.py:493
  27.0 14.3 %collective-permute-start.21 = (bf16[24,2048]{1,0:T(8,128)(2,1)S(1)}, bf16[24,2048]{1,0:T(8,128)(2,1)S(1)}, u32[]{:S(2)}, u32[]{:S(2)}) collective-permute-start(bf16[24,2048]{1,0:T(8,128)(2,1)S(1)} %copy-done.31), channel_id=1, source_target_pairs={{0,4},{4,0},{8,12},{12,8},{16,20},{20,16},{24,28},{28,24},{1,5},{5... | collective-permute-start | bytes 294920 | tf_op jit(solution)/shard_map/ppermute | solution.py:516
  28.9 25.1 %collective-permute-start.22 = (bf16[24,2048]{1,0:T(8,128)(2,1)S(1)}, bf16[24,2048]{1,0:T(8,128)(2,1)S(1)}, u32[]{:S(2)}, u32[]{:S(2)}) collective-permute-start(bf16[24,2048]{1,0:T(8,128)(2,1)S(1)} %copy-done.29), channel_id=1, source_target_pairs={{0,8},{4,12},{8,0},{12,4},{16,24},{20,28},{24,16},{28,20},{1,9},{5... | collective-permute-start | bytes 294920 | tf_op jit(solution)/shard_map/ppermute | solution.py:516
  41.3 18.4 %collective-permute-start.23 = (bf16[24,2048]{1,0:T(8,128)(2,1)S(1)}, bf16[24,2048]{1,0:T(8,128)(2,1)S(1)}, u32[]{:S(2)}, u32[]{:S(2)}) collective-permute-start(bf16[24,2048]{1,0:T(8,128)(2,1)S(1)} %copy-done.27), channel_id=1, source_target_pairs={{0,12},{4,8},{8,4},{12,0},{16,28},{20,24},{24,20},{28,16},{1,13},{... | collective-permute-start | bytes 294920 | tf_op jit(solution)/shard_map/ppermute | solution.py:516
  54.1 15.8 %collective-permute-start.24 = (bf16[24,2048]{1,0:T(8,128)(2,1)S(1)}, bf16[24,2048]{1,0:T(8,128)(2,1)S(1)}, u32[]{:S(2)}, u32[]{:S(2)}) collective-permute-start(bf16[24,2048]{1,0:T(8,128)(2,1)S(1)} %copy-done.24), channel_id=1, source_target_pairs={{0,16},{4,20},{8,24},{12,28},{16,0},{20,4},{24,8},{28,12},{1,17},{... | collective-permute-start | bytes 294920 | tf_op jit(solution)/shard_map/ppermute | solution.py:516
  59.7 12.0 %collective-permute-start.25 = (bf16[24,2048]{1,0:T(8,128)(2,1)S(1)}, bf16[24,2048]{1,0:T(8,128)(2,1)S(1)}, u32[]{:S(2)}, u32[]{:S(2)}) collective-permute-start(bf16[24,2048]{1,0:T(8,128)(2,1)S(1)} %copy-done.23), channel_id=1, source_target_pairs={{0,20},{4,16},{8,28},{12,24},{16,4},{20,0},{24,12},{28,8},{1,21},{... | collective-permute-start | bytes 294920 | tf_op jit(solution)/shard_map/ppermute | solution.py:516
  69.9 22.3 %collective-permute-start.1 = (bf16[256,2048]{1,0:T(8,128)(2,1)}, bf16[256,2048]{1,0:T(8,128)(2,1)}, u32[]{:S(2)}, u32[]{:S(2)}) collective-permute-start(bf16[256,2048]{1,0:T(8,128)(2,1)} %r_1_.2), channel_id=1, source_target_pairs={{0,2},{1,3},{2,0},{3,1},{4,6},{5,7},{6,4},{7,5},{8,10},{9,11},{10,... | collective-permute-start | bytes 3145736 | tf_op jit(solution)/shard_map/ppermute | solution.py:487
  85.5 15.7 %collective-permute-start = (bf16[256,2048]{1,0:T(8,128)(2,1)}, bf16[256,2048]{1,0:T(8,128)(2,1)}, u32[]{:S(2)}, u32[]{:S(2)}) collective-permute-start(bf16[256,2048]{1,0:T(8,128)(2,1)} %r_1_.2), channel_id=1, source_target_pairs={{0,1},{1,0},{2,3},{3,2},{4,5},{5,4},{6,7},{7,6},{8,9},{9,8},{10,11... | collective-permute-start | bytes 3145736 | tf_op jit(solution)/shard_map/ppermute | solution.py:488
  92.2 73.2 %collective-permute-start.13 = (bf16[2048,128]{1,0:T(8,128)(2,1)S(1)}, bf16[2048,128]{1,0:T(8,128)(2,1)}, u32[]{:S(2)}, u32[]{:S(2)}) collective-permute-start(bf16[2048,128]{1,0:T(8,128)(2,1)S(1)} %copy-done.4), channel_id=1, source_target_pairs={{0,1},{1,0},{2,3},{3,2},{4,5},{5,4},{6,7},{7,6},{8,9},{9,8},{10,11... | collective-permute-start | bytes 1572872 | tf_op jit(solution)/shard_map/ppermute | solution.py:491
  92.2 77.5 %collective-permute-start.14 = (bf16[2048,128]{1,0:T(8,128)(2,1)S(1)}, bf16[2048,128]{1,0:T(8,128)(2,1)S(1)}, u32[]{:S(2)}, u32[]{:S(2)}) collective-permute-start(bf16[2048,128]{1,0:T(8,128)(2,1)S(1)} %copy-done.5), channel_id=1, source_target_pairs={{0,1},{1,0},{2,3},{3,2},{4,5},{5,4},{6,7},{7,6},{8,9},{9,8},{10,11... | collective-permute-start | bytes 1572872 | tf_op jit(solution)/shard_map/ppermute | solution.py:491
  92.7 23.0 %collective-permute-start.28 = (bf16[192,2048]{1,0:T(8,128)(2,1)}, bf16[192,2048]{1,0:T(8,128)(2,1)S(1)}, u32[]{:S(2)}, u32[]{:S(2)}) collective-permute-start(bf16[192,2048]{1,0:T(8,128)(2,1)} %near_join.1.refs_0_), channel_id=1, source_target_pairs={{0,2},{1,3},{2,0},{3,1},{4,6},{5,7},{6,4},{7,5},{8,10},{9,11},{10,... | collective-permute-start | bytes 2359304 | tf_op jit(solution)/shard_map/ppermute | solution.py:658
  94.2 45.0 %collective-permute-start.2 = (bf16[256,2048]{1,0:T(8,128)(2,1)}, bf16[256,2048]{1,0:T(8,128)(2,1)}, u32[]{:S(2)}, u32[]{:S(2)}) collective-permute-start(bf16[256,2048]{1,0:T(8,128)(2,1)} %collective-permute-done.1.r_1_), channel_id=1, source_target_pairs={{0,1},{1,0},{2,3},{3,2},{4,5},{5,4},{6,7},{7,6},{8,9},{9,8},{10,11... | collective-permute-start | bytes 3145736 | tf_op jit(solution)/shard_map/ppermute | solution.py:489
  101.3 28.2 %collective-permute-start.20 = (bf16[192,2048]{1,0:T(8,128)(2,1)}, bf16[192,2048]{1,0:T(8,128)(2,1)}, u32[]{:S(2)}, u32[]{:S(2)}) collective-permute-start(bf16[192,2048]{1,0:T(8,128)(2,1)} %get-tuple-element.61), channel_id=1, source_target_pairs={{0,2},{1,3},{2,0},{3,1},{4,6},{5,7},{6,4},{7,5},{8,10},{9,11},{10,... | collective-permute-start | bytes 2359304 | tf_op jit(solution)/shard_map/ppermute | solution.py:674
  115.7 55.3 %collective-permute-start.15 = (bf16[128,2048]{1,0:T(8,128)(2,1)S(1)}, bf16[128,2048]{1,0:T(8,128)(2,1)}, u32[]{:S(2)}, u32[]{:S(2)}) collective-permute-start(bf16[128,2048]{1,0:T(8,128)(2,1)S(1)} %copy-done.6), channel_id=1, source_target_pairs={{0,1},{1,0},{2,3},{3,2},{4,5},{5,4},{6,7},{7,6},{8,9},{9,8},{10,11... | collective-permute-start | bytes 1572872 | tf_op jit(solution)/shard_map/ppermute | solution.py:491
  129.4 58.6 %collective-permute-start.29 = (bf16[192,2048]{1,0:T(8,128)(2,1)}, bf16[192,2048]{1,0:T(8,128)(2,1)}, u32[]{:S(2)}, u32[]{:S(2)}) collective-permute-start(bf16[192,2048]{1,0:T(8,128)(2,1)} %get-tuple-element.71), channel_id=1, source_target_pairs={{0,2},{1,3},{2,0},{3,1},{4,6},{5,7},{6,4},{7,5},{8,10},{9,11},{10,... | collective-permute-start | bytes 2359304 | tf_op jit(solution)/shard_map/ppermute | solution.py:662
  133.3 80.3 %all-to-all-start.1 = ((bf16[8,24,2048]{2,1,0:T(8,128)(2,1)}), bf16[8,24,2048]{2,1,0:T(8,128)(2,1)S(1)}, u32[]{:S(2)}, u32[]{:S(2)}) async-start(bf16[8,24,2048]{2,1,0:T(8,128)(2,1)} %bitcast.15), calls=%async_computation.1 | async-start | bytes 1572864 | tf_op jit(solution)/shard_map/all_to_all | solution.py:523
  161.5 15.1 %collective-permute-start.4 = (bf16[144,256]{1,0:T(8,128)(2,1)}, bf16[144,256]{1,0:T(8,128)(2,1)S(1)}, u32[]{:S(2)}, u32[]{:S(2)}) collective-permute-start(bf16[144,256]{1,0:T(8,128)(2,1)} %shard_map.224), channel_id=1, source_target_pairs={{0,8},{4,12},{8,16},{12,20},{16,24},{20,28},{1,9},{5,13},{9,17},{1... | collective-permute-start | bytes 221192 | tf_op jit(solution)/shard_map/ppermute | solution.py:623
  165.4 11.2 %collective-permute-start.5 = (bf16[144,256]{1,0:T(8,128)(2,1)}, bf16[144,256]{1,0:T(8,128)(2,1)S(1)}, u32[]{:S(2)}, u32[]{:S(2)}) collective-permute-start(bf16[144,256]{1,0:T(8,128)(2,1)} %shard_map.224), channel_id=1, source_target_pairs={{0,16},{4,20},{8,24},{12,28},{1,17},{5,21},{9,25},{13,29},{2,18},{... | collective-permute-start | bytes 221192 | tf_op jit(solution)/shard_map/ppermute | solution.py:623
  176.1 15.6 %collective-permute-start.16 = (bf16[128,2048]{1,0:T(8,128)(2,1)}, bf16[128,2048]{1,0:T(8,128)(2,1)S(1)}, u32[]{:S(2)}, u32[]{:S(2)}) collective-permute-start(bf16[128,2048]{1,0:T(8,128)(2,1)} %get-tuple-element.58), channel_id=1, source_target_pairs={{0,2},{1,3},{2,0},{3,1},{4,6},{5,7},{6,4},{7,5},{8,10},{9,11},{10,... | collective-permute-start | bytes 1572872 | tf_op jit(solution)/shard_map/ppermute | solution.py:660
  181.6 13.6 %collective-permute-start.8 = (bf16[256,512]{1,0:T(8,128)(2,1)}, bf16[256,512]{1,0:T(8,128)(2,1)S(1)}, u32[]{:S(2)}, u32[]{:S(2)}) collective-permute-start(bf16[256,512]{1,0:T(8,128)(2,1)} %get-tuple-element.51), channel_id=1, source_target_pairs={{0,2},{1,3},{2,0},{3,1},{4,6},{5,7},{6,4},{7,5},{8,10},{9,11},{10,... | collective-permute-start | bytes 786440 | tf_op jit(solution)/shard_map/ppermute | solution.py:654
  183.0 13.1 %collective-permute-start.9 = (bf16[256,512]{1,0:T(8,128)(2,1)}, bf16[256,512]{1,0:T(8,128)(2,1)S(1)}, u32[]{:S(2)}, u32[]{:S(2)}) collective-permute-start(bf16[256,512]{1,0:T(8,128)(2,1)} %get-tuple-element.52), channel_id=1, source_target_pairs={{0,3},{1,2},{2,1},{3,0},{4,7},{5,6},{6,5},{7,4},{8,11},{9,10},{10,... | collective-permute-start | bytes 786440 | tf_op jit(solution)/shard_map/ppermute | solution.py:654
  195.2 15.3 %collective-permute-start.32 = (bf16[24,2048]{1,0:T(8,128)(2,1)}, bf16[24,2048]{1,0:T(8,128)(2,1)S(1)}, u32[]{:S(2)}, u32[]{:S(2)}) collective-permute-start(bf16[24,2048]{1,0:T(8,128)(2,1)} %get-tuple-element.75), channel_id=1, source_target_pairs={{0,12},{4,8},{8,4},{12,0},{16,28},{20,24},{24,20},{28,16},{1,13},{... | collective-permute-start | bytes 294920 | tf_op jit(solution)/shard_map/ppermute | solution.py:516
  196.2 14.7 %collective-permute-start.33 = (bf16[24,2048]{1,0:T(8,128)(2,1)}, bf16[24,2048]{1,0:T(8,128)(2,1)S(1)}, u32[]{:S(2)}, u32[]{:S(2)}) collective-permute-start(bf16[24,2048]{1,0:T(8,128)(2,1)} %get-tuple-element.76), channel_id=1, source_target_pairs={{0,16},{4,20},{8,24},{12,28},{16,0},{20,4},{24,8},{28,12},{1,17},{... | collective-permute-start | bytes 294920 | tf_op jit(solution)/shard_map/ppermute | solution.py:516
  196.2 17.4 %collective-permute-start.34 = (bf16[24,2048]{1,0:T(8,128)(2,1)}, bf16[24,2048]{1,0:T(8,128)(2,1)S(1)}, u32[]{:S(2)}, u32[]{:S(2)}) collective-permute-start(bf16[24,2048]{1,0:T(8,128)(2,1)} %get-tuple-element.77), channel_id=1, source_target_pairs={{0,20},{4,16},{8,28},{12,24},{16,4},{20,0},{24,12},{28,8},{1,21},{... | collective-permute-start | bytes 294920 | tf_op jit(solution)/shard_map/ppermute | solution.py:516
  200.0 13.5 %collective-permute-start.35 = (bf16[24,2048]{1,0:T(8,128)(2,1)}, bf16[24,2048]{1,0:T(8,128)(2,1)S(1)}, u32[]{:S(2)}, u32[]{:S(2)}) collective-permute-start(bf16[24,2048]{1,0:T(8,128)(2,1)} %get-tuple-element.78), channel_id=1, source_target_pairs={{0,24},{4,28},{8,16},{12,20},{16,8},{20,12},{24,0},{28,4},{1,25},{... | collective-permute-start | bytes 294920 | tf_op jit(solution)/shard_map/ppermute | solution.py:516
  200.6 13.0 %collective-permute-start.36 = (bf16[24,2048]{1,0:T(8,128)(2,1)}, bf16[24,2048]{1,0:T(8,128)(2,1)S(1)}, u32[]{:S(2)}, u32[]{:S(2)}) collective-permute-start(bf16[24,2048]{1,0:T(8,128)(2,1)} %get-tuple-element.79), channel_id=1, source_target_pairs={{0,28},{4,24},{8,20},{12,16},{16,12},{20,8},{24,4},{28,0},{1,29},{... | collective-permute-start | bytes 294920 | tf_op jit(solution)/shard_map/ppermute | solution.py:516
  (48 other events, 602.5 us)
where the time goes:
time: 220 us; the launch traced here: 218 us
  Pallas kernels  81 us (37%)
  waiting for transfers between devices  64.8 us (29%)
  starting transfers between devices  64.2 us (29%)
  local copies, waits for them, and re-layouts  6.18 us (3%)
    ppermute x14, waiting for transfers between devices, swap(): lax.ppermute(pieces[n], 'ep', [(e, e ^ n) for e in range(ep_count)])  42.9 us
    pallas_call x2, Pallas kernels, local_part(): pl.pallas_call(lambda *r: local_kernel(heads, *r), grid_spec=pltpu.Prefet...  27.6 us
    ppermute x14, starting transfers between devices, swap(): lax.ppermute(pieces[n], 'ep', [(e, e ^ n) for e in range(ep_count)])  26.4 us
    pallas_call x3, Pallas kernels, ffn(): pl.pallas_call(lambda *refs: ffn_kernel(arrays, slots, *refs), grid=(step...  19 us
    all_to_all x2, starting transfers between devices, exchange(): out = lax.all_to_all(cut, 'ep', split_axis=0, concat_axis=0, tiled=True)  12.1 us
    ppermute x3, starting transfers between devices, body(): lax.ppermute(pair, 'ep', [(e, e + 2 * s) for e in range(ep_count - 2 * s)])  9.45 us
    pallas_call x2, Pallas kernels, gated_part(): pl.pallas_call(lambda *r: gated_kernel(heads, tp_count, first_slot, *r),...  8.52 us
    ppermute x1, waiting for transfers between devices, body(): picks_x = lax.ppermute(picks, 'tp', across)  7.67 us
  transfers between devices with their start and end apart: 39, of which 14 were waited for; matrix products, arithmetic and copies ran while one was open for 1% of the time, Pallas kernels for 34%

commit v1 on v0

--- a/solution.py
+++ b/solution.py
@@ -15,8 +15,8 @@
 bf16 = jnp.bfloat16
 
 
-def params(**kw):
-    return pltpu.CompilerParams(**kw)
+def params(mib=None):
+    return pltpu.CompilerParams(vmem_limit_bytes=None if mib is None else mib * 1024 * 1024)
 
 
 def cost(flops, nbytes):
@@ -77,27 +77,28 @@
     return jnp.where(chosen, 1.0, 0.0).astype(bf16), jnp.where(chosen, weight_at, 0.0)
 
 
-def pack_own_kernel(experts, slots, place_ref, x_ref, gain_ref, picks_ref, factor_ref, *refs):
-    normed_ref, weight_ref = refs[:2]
-    outs = refs[2:]
+def row_blocks(rows, slots, groups):
+    row = lax.broadcasted_iota(jnp.int32, (rows, 1), 0)
+    block = jnp.zeros(row.shape, jnp.int32)
+    for n in range(1, groups):
+        block = block + jnp.where(row >= n * slots, 1, 0)
+    return row, block
+
+
+def pack_own_kernel(
+    experts, slots, groups, place_ref, x_ref, gain_ref, picks_ref, factor_ref, *outs
+):
+    normed_ref, weight_ref, out_ref = outs
     normed = rms_rows(x_ref[...], gain_ref[...])
     normed_ref[...] = normed
-    row = lax.broadcasted_iota(jnp.int32, (weight_ref.shape[0], 1), 0)
-    block = jnp.zeros(row.shape, jnp.int32)
-    for n in range(1, len(outs)):
-        block = block + jnp.where(row >= n * slots, 1, 0)
+    row, block = row_blocks(weight_ref.shape[0], slots, groups)
+    local = experts // groups
+    place = (row - block * slots).astype(f32)
+    picks, factors = picks_ref[...].astype(f32), factor_ref[...]
+    pick, _ = slot_choice(picks, factors, (block * local).astype(f32), place, experts)
     owner = jnp.bitwise_xor(block, place_ref[0])
-    local = experts // len(outs)
-    pick, weights = slot_choice(
-        picks_ref[...].astype(f32),
-        factor_ref[...],
-        (owner * local).astype(f32),
-        (row - block * slots).astype(f32),
-        experts,
-    )
-    rows = dot(pick, normed).astype(bf16)
-    for n, ref in enumerate(outs):
-        ref[...] = rows[n * slots : (n + 1) * slots]
+    _, weights = slot_choice(picks, factors, (owner * local).astype(f32), place, experts)
+    out_ref[...] = dot(pick, normed).astype(bf16)
     weight_ref[...] = weights
 
 
@@ -117,10 +118,7 @@
     weight_ref,
 ):
     tok_ref[...] = rms_rows(x_ref[...], gain_ref[...])
-    row = lax.broadcasted_iota(jnp.int32, (weight_ref.shape[0], 1), 0)
-    block = jnp.zeros(row.shape, jnp.int32)
-    for n in range(1, groups):
-        block = block + jnp.where(row >= n * slots, 1, 0)
+    row, block = row_blocks(weight_ref.shape[0], slots, groups)
     local = experts // groups
     tables = ((block * local + 1).astype(f32), (row - block * slots).astype(f32))
     own, weights = slot_choice(picks_ref[...].astype(f32), factor_ref[...], *tables, experts)
@@ -134,20 +132,20 @@
             ]
 
 
-def ffn_kernel(arrays, slots, *refs):
+def ffn_kernel(arrays, expert, slots, *refs):
     ins = refs[:arrays]
     weights = refs[arrays : arrays + 6]
     outs = refs[arrays + 6 :]
+    height = ins[0].shape[0]
     rows = jnp.concatenate([r[...] for r in ins], axis=0)
     total = None
     for n in range(2):
-        gate_w, up_w, down_w = (w[...] for w in weights[3 * n : 3 * n + 3])
-        if len(gate_w.shape) == 3:
-            gate_w, up_w, down_w = gate_w[0], up_w[0], down_w[0]
+        gate_w, up_w, down_w = (
+            w[...] if len(w.shape) == 2 else w[expert] for w in weights[3 * n : 3 * n + 3]
+        )
         hidden = (silu(dot(rows, gate_w)) * dot(rows, up_w)).astype(bf16)
         part = dot(hidden, down_w)
         total = part if total is None else total + part
-    height = ins[0].shape[0]
     if len(outs) == arrays:
         for k in range(arrays):
             outs[k][...] = total[k * height : (k + 1) * height].astype(bf16)
@@ -158,48 +156,47 @@
             outs[k][n * slots : (n + 1) * slots] = piece
 
 
-def ffn(rows, weights, expert, steps, slots=None):
+def ffn(rows, weights, expert, slots=None, grant=None):
     arrays = len(rows)
     count, width = rows[0].shape
-    height = count // steps
-    row_spec = pl.BlockSpec((height, width), lambda i: (i, 0))
-    if expert is None:
-        weight_specs = [pl.BlockSpec(w.shape, lambda i: (0, 0)) for w in weights]
-        inner = 2 * weights[0].shape[1]
-    else:
+    inner = weights[0].shape[-1]
+    outs = 2
+    out = jax.ShapeDtypeStruct((arrays * count // outs, width), bf16)
+    held = expert
+    if grant is None and expert is not None:
+        held = 0
         weight_specs = [
             pl.BlockSpec((1,) + w.shape[1:], lambda i: (expert, 0, 0)) for w in weights
         ]
-        inner = 2 * weights[0].shape[2]
-    if slots is None:
-        outs, parts = arrays, 1
     else:
-        outs, parts = 2, 2
-    out = jax.ShapeDtypeStruct((count // parts, width), bf16)
+        weight_specs = vmem(6)
     return pl.pallas_call(
-        lambda *refs: ffn_kernel(arrays, slots, *refs),
-        grid=(steps,),
-        in_specs=[row_spec] * arrays + weight_specs,
-        out_specs=[pl.BlockSpec((height // parts, width), lambda i: (i, 0))] * outs,
+        lambda *refs: ffn_kernel(arrays, held, slots, *refs),
+        grid=(1,),
+        in_specs=vmem(arrays) + weight_specs,
+        out_specs=vmem(outs),
         out_shape=[out] * outs,
-        compiler_params=params(),
+        compiler_params=params(grant),
         cost_estimate=cost(
-            6 * arrays * count * width * inner, 4 * arrays * count * width + 6 * width * inner
+            12 * arrays * count * width * inner, 4 * arrays * count * width + 12 * width * inner
         ),
     )(*rows, *weights)
 
 
-def join_kernel(*refs):
-    height = refs[0].shape[0]
-    for n, ref in enumerate(refs[:-1]):
-        refs[-1][n * height : (n + 1) * height, :] = ref[...]
-
-
-def sum_kernel(a_ref, b_ref, *outs):
+def sum_kernel(a_ref, b_ref, out_ref):
+    out_ref[...] = (a_ref[...].astype(f32) + b_ref[...].astype(f32)).astype(bf16)
+
+
+def sum_swap_kernel(slots, place_ref, a_ref, b_ref, *outs):
     total = (a_ref[...].astype(f32) + b_ref[...].astype(f32)).astype(bf16)
-    height = outs[0].shape[0]
+    rows = total.shape[0]
+    row, block = row_blocks(rows, slots, len(outs))
+    wanted = jnp.bitwise_xor(block, place_ref[0]) * slots + row - block * slots
+    column = lax.broadcasted_iota(jnp.int32, (rows, rows), 1)
+    pick = jnp.where(column == wanted, 1.0, 0.0).astype(bf16)
+    total = dot(pick, total).astype(bf16)
     for n, ref in enumerate(outs):
-        ref[...] = total[n * height : (n + 1) * height]
+        ref[...] = total[n * slots : (n + 1) * slots]
 
 
 def finish_kernel(near_weight_ref, far_weight_ref, shared_ref, got_ref, far_ref, *refs):
@@ -230,28 +227,17 @@
         in_specs=specs,
         out_specs=out_specs,
         out_shape=outs,
-        compiler_params=params(),
+        compiler_params=params(12),
         cost_estimate=cost(flops, sum(a.size * a.dtype.itemsize for a in ins)),
     )(*ins)
 
 
-def local_kernel(heads, place_ref, first_ref, second_ref, *refs):
-    (
-        gain_ref,
-        q_ref,
-        k_ref,
-        d_ref,
-        v_ref,
-        g_ref,
-        shift_ref,
-        fade_ref,
-        out_ref,
-        qg_ref,
-        gate_ref,
-        pack_ref,
-        buffer,
-        sems,
-    ) = refs
+def local_kernel(heads, carried, place_ref, first_ref, second_ref, *refs):
+    gain_ref, shift_ref, fade_ref = refs[:3]
+    weight_refs = refs[3:8]
+    out_ref, qg_ref, gate_ref, pack_ref = refs[8 + carried : 12 + carried]
+    buffer, sems = refs[12 + carried :]
+    d_ref, k_ref, q_ref, v_ref, g_ref = weight_refs
     slot = pl.program_id(0)
     span = SPAN_LENGTH
     key_width = q_ref.shape[1]
@@ -265,9 +251,9 @@
     pltpu.make_async_copy(first_ref, buffer.at[slot], sems.at[slot]).wait()
     normed = rms_rows(buffer[slot], gain_ref[...])
     rows = normed.shape[0]
+    logits = dot(normed, d_ref[...]).astype(bf16).astype(f32) + shift_ref[...]
+    keys = dot(normed, k_ref[...]).astype(bf16).astype(f32)
     query = dot(normed, q_ref[...]).astype(bf16).astype(f32) * MATCHER_WIDTH ** (-0.5)
-    keys = dot(normed, k_ref[...]).astype(bf16).astype(f32)
-    logits = dot(normed, d_ref[...]).astype(bf16).astype(f32) + shift_ref[...]
     value = dot(normed, v_ref[...]).astype(bf16)
     gate_ref[0] = dot(normed, g_ref[...]).astype(bf16)
 
@@ -275,8 +261,7 @@
     head_lane = lax.broadcasted_iota(jnp.int32, (heads, key_width), 1)
     low = head_row * MATCHER_WIDTH
     spread = jnp.where((head_lane >= low) & (head_lane < low + MATCHER_WIDTH), 1.0, 0.0).astype(bf16)
-    f1, f2, f3 = split_three(fade_ref[...])
-    fade = dot(f1, spread) + dot(f2, spread) + dot(f3, spread)
+    fade = sum(dot(part, spread, ((0,), (0,))) for part in split_three(fade_ref[...]))
     soft = jnp.minimum(logits, 0.0) - jnp.log1p(jnp.exp(-jnp.abs(logits)))
     rate = soft / GATE_SOFTNESS + fade
 
@@ -343,64 +328,43 @@
     return held * pack[DV : DV + 1].astype(f32) + pack[0:DV].astype(f32)
 
 
-def store_pack(ref, held, fading):
-    ref[0:DV, :] = held.astype(bf16)
-    ref[DV:, :] = jnp.broadcast_to(fading, (ref.shape[0] - DV, fading.shape[1])).astype(bf16)
-
-
-def block_pack(packs, slot):
-    inner = jnp.bitwise_and(slot, 1)
-    return jnp.where(slot >= 2, packs[1][inner], packs[0][inner])
-
-
-def chain_kernel(blocks, place_ref, first_ref, second_ref, out_ref):
+def chain_kernel(blocks, place_ref, packs_ref, out_ref):
     held = None
     for n in range(blocks):
-        pack = block_pack((first_ref, second_ref), jnp.bitwise_xor(place_ref[1], n))
+        pack = packs_ref[jnp.bitwise_xor(place_ref[1], n)]
         if held is None:
             held, fading = pack[0:DV], pack[DV : DV + 1]
         else:
             held, fading = follow(held, pack), fading * pack[DV : DV + 1]
-    store_pack(out_ref, held, fading)
-
-
-def pair_kernel(place_ref, own_ref, got_ref, out_ref):
-    own, got = own_ref[...].astype(f32), got_ref[...].astype(f32)
-    odd = jnp.bitwise_and(place_ref[0], 1) == 1
-    earlier, later = jnp.where(odd, got, own), jnp.where(odd, own, got)
-    store_pack(
-        out_ref, follow(earlier[0:DV], later), earlier[DV : DV + 1] * later[DV : DV + 1]
-    )
+    held = held.astype(bf16)
+    fading = jnp.broadcast_to(fading, (out_ref.shape[1] - DV, fading.shape[1])).astype(bf16)
+    for n in range(out_ref.shape[0]):
+        out_ref[n, 0:DV, :] = held
+        out_ref[n, DV:, :] = fading
 
 
 def gated_kernel(
     heads,
     blocks,
-    first_slot,
     place_ref,
     local_ref,
     qg_ref,
     gate_ref,
     gain_ref,
     start_ref,
-    pack_a_ref,
-    pack_b_ref,
-    even_ref,
+    block_ref,
+    pack_ref,
     *refs,
 ):
-    outs = refs[-3:-1]
-    packs = refs[:-3]
+    outs = refs[:-1]
     entering = refs[-1]
     key_width = qg_ref.shape[2]
 
     @pl.when(pl.program_id(0) == 0)
     def _():
-        held = start_ref[...]
-        pair = jnp.right_shift(place_ref[0], 1)
-        for shift in range(len(packs), 0, -1):
-            held = jnp.where(pair >= shift, follow(held, packs[shift - 1][...]), held)
-        odd = jnp.bitwise_and(place_ref[0], 1) == 1
-        held = jnp.where(odd, follow(held, even_ref[...]), held)
+        held = start_ref[...].T
+        for n in range(pack_ref.shape[0]):
+            held = jnp.where(place_ref[0] > n, follow(held, pack_ref[n]), held)
         width_bits = MATCHER_WIDTH.bit_length() - 1
         lane_head = jnp.right_shift(
             lax.broadcasted_iota(jnp.int32, (DV, key_width), 1), width_bits
@@ -411,9 +375,9 @@
                 entering[slot, h * DV : (h + 1) * DV, :] = jnp.where(
                     lane_head == h, held, 0.0
                 ).astype(bf16)
-            held = follow(held, block_pack((pack_a_ref, pack_b_ref), slot))
-
-    slot = pl.program_id(0) + first_slot
+            held = follow(held, block_ref[slot])
+
+    slot = jnp.bitwise_xor(pl.program_id(0), blocks // 2)
     attended = local_ref[0] + dot(qg_ref[0], entering[slot], ((1,), (1,)))
     parts = []
     for h in range(heads):
@@ -425,20 +389,18 @@
     rows = jnp.concatenate(parts, axis=1)
     for n, ref in enumerate(outs):
 
-        @pl.when(pl.program_id(0) == n)
+        @pl.when(slot == n)
         def _(ref=ref):
             ref[...] = rows
 
 
-def project_kernel(groups, place_ref, *refs):
-    w_ref, out_ref = refs[groups:]
-    width = refs[0].shape[1]
-    total = None
-    for n in range(groups):
-        first = pl.multiple_of(jnp.bitwise_xor(place_ref[0], n) * width, width)
-        part = dot(refs[n][...], w_ref[pl.ds(first, width), :])
-        total = part if total is None else total + part
-    out_ref[...] = total.astype(bf16)
+def project_kernel(place_ref, first_ref, second_ref, *refs):
+    weights = refs[0:2]
+    out_ref = refs[-1]
+    total = dot(first_ref[...], weights[0][...]) + dot(second_ref[...], weights[1][...])
+    if len(refs) == 4:
+        total = total + refs[2][...]
+    out_ref[...] = total.astype(out_ref.dtype)
 
 
 def body(
@@ -497,15 +459,15 @@
     moe_gain = specialist_gain_vector.reshape(1, -1)
     piece = jax.ShapeDtypeStruct((slots, feature_width), bf16)
     smem = [pl.BlockSpec(memory_space=pltpu.SMEM)]
-    normed, near_weight, *near_out = pl.pallas_call(
-        lambda *r: pack_own_kernel(experts, slots, *r),
+    normed, near_weight, near_out = pl.pallas_call(
+        lambda *r: pack_own_kernel(experts, slots, ep_count, *r),
         in_specs=smem + vmem(4),
-        out_specs=vmem(2 + ep_count),
+        out_specs=vmem(3),
         out_shape=[
             jax.ShapeDtypeStruct((tokens, feature_width), bf16),
             jax.ShapeDtypeStruct((near, tokens), f32),
-        ]
-        + [piece] * ep_count,
+            jax.ShapeDtypeStruct((near, feature_width), bf16),
+        ],
         compiler_params=params(),
         cost_estimate=cost(2e9, 4e6),
         name="pack_own",
@@ -523,15 +485,7 @@
         out = lax.all_to_all(cut, "ep", split_axis=0, concat_axis=0, tiled=True)
         return out.reshape(shape)
 
-    near_in = pl.pallas_call(
-        join_kernel,
-        in_specs=vmem(ep_count),
-        out_specs=pl.BlockSpec(memory_space=pltpu.VMEM),
-        out_shape=jax.ShapeDtypeStruct((near, feature_width), bf16),
-        compiler_params=params(),
-        cost_estimate=cost(1e9, 2e6),
-        name="near_join",
-    )(*swap(near_out))
+    near_in = exchange(near_out)
 
     normed_x, far_out, far_weight = pl.pallas_call(
         lambda *r: pack_both_kernel(experts, slots, ep_count, *r),
@@ -563,114 +517,96 @@
     pack_rows = DV + 16
     place = jnp.concatenate([ep_place, tp_place])
     whole = lambda a: pl.BlockSpec(a.shape, lambda i, *_: (0,) * len(a.shape))
-    by_slot = lambda r, w: pl.BlockSpec((1, r, w), lambda i, *_: (i, 0, 0))
     mix_gain = mixer_gain_vector.reshape(1, -1)
     shift = fading_shift_vector.reshape(1, -1)
-    weights = (asker_matrix, matcher_matrix, fading_matrix, content_matrix, result_valve_matrix)
-
-    def local_part(raws, first_slot):
+    weights = (fading_matrix, matcher_matrix, asker_matrix, content_matrix, result_valve_matrix)
+    fade = extra_fade_amount.T
+    any_space = pl.BlockSpec(memory_space=pl.ANY)
+
+    def local_part(raws, first_slot, carried=()):
         fade_spec = pl.BlockSpec(
-            (rows, heads), lambda i, p: (jnp.bitwise_xor(i + first_slot, p[1]), 0)
+            (heads, rows), lambda i, p: (0, jnp.bitwise_xor(i + first_slot, p[1]))
         )
+        by_slot = lambda r, w: pl.BlockSpec((1, r, w), lambda i, p: (i + first_slot, 0, 0))
+        shapes = [
+            jax.ShapeDtypeStruct((tp_count, rows, value_width), f32),
+            jax.ShapeDtypeStruct((tp_count, rows, key_width), bf16),
+            jax.ShapeDtypeStruct((tp_count, rows, value_width), bf16),
+            jax.ShapeDtypeStruct((tp_count, pack_rows, key_width), f32),
+        ]
         return pl.pallas_call(
-            lambda *r: local_kernel(heads, *r),
+            lambda *r: local_kernel(heads, len(carried), *r),
             grid_spec=pltpu.PrefetchScalarGridSpec(
                 num_scalar_prefetch=1,
                 grid=(2,),
-                in_specs=[pl.BlockSpec(memory_space=pl.ANY)] * 2
-                + [whole(mix_gain)]
-                + [whole(w) for w in weights]
-                + [whole(shift), fade_spec],
-                out_specs=[
-                    by_slot(rows, value_width),
-                    by_slot(rows, key_width),
-                    by_slot(rows, value_width),
-                    by_slot(pack_rows, key_width),
-                ],
+                in_specs=[any_space] * 2
+                + [whole(mix_gain), whole(shift), fade_spec]
+                + vmem(5)
+                + [any_space] * len(carried),
+                out_specs=[by_slot(*shape.shape[1:]) for shape in shapes],
                 scratch_shapes=[
                     pltpu.VMEM((2, rows, feature_width), bf16),
                     pltpu.SemaphoreType.DMA((2,)),
                 ],
             ),
-            out_shape=[
-                jax.ShapeDtypeStruct((2, rows, value_width), f32),
-                jax.ShapeDtypeStruct((2, rows, key_width), bf16),
-                jax.ShapeDtypeStruct((2, rows, value_width), bf16),
-                jax.ShapeDtypeStruct((2, pack_rows, key_width), f32),
-            ],
+            out_shape=shapes,
+            input_output_aliases={11 + n: n for n in range(len(carried))},
             compiler_params=params(),
             cost_estimate=cost(1e10, 1e7),
-        )(place, *raws, mix_gain, *weights, shift, extra_fade_amount)
-
-    *part_a, pack_a = local_part((mixer_microbatch, mix_raw_c), 0)
-    *part_b, pack_b = local_part((mix_raw_x, mix_raw_xc), 2)
-    pack_shape = jax.ShapeDtypeStruct((pack_rows, key_width), bf16)
-
-    def small_call(kernel, ins):
-        return pl.pallas_call(
-            kernel,
-            in_specs=smem + vmem(len(ins)),
-            out_specs=pl.BlockSpec(memory_space=pltpu.VMEM),
-            out_shape=pack_shape,
-            compiler_params=params(),
-            cost_estimate=cost(1e9, 1e6),
-        )(place, *ins)
-
-    pack = small_call(lambda *r: chain_kernel(tp_count, *r), (pack_a, pack_b))
-    got = lax.ppermute(pack, "ep", [(e, e ^ 1) for e in range(ep_count)])
-    pair = small_call(pair_kernel, (pack, got))
-    packs = [
-        lax.ppermute(pair, "ep", [(e, e + 2 * s) for e in range(ep_count - 2 * s)])
-        for s in range(1, ep_count // 2)
-    ]
-    start = starting_memory.T
+        )(place, *raws, mix_gain, shift, fade, *weights, *carried)
+
+    local = local_part((mixer_microbatch, mix_raw_c), 0)
+    *local, block_packs = local_part((mix_raw_x, mix_raw_xc), 2, local)
+    pack = pl.pallas_call(
+        lambda *r: chain_kernel(tp_count, *r),
+        in_specs=smem + vmem(1),
+        out_specs=pl.BlockSpec(memory_space=pltpu.VMEM),
+        out_shape=jax.ShapeDtypeStruct((ep_count, pack_rows, key_width), bf16),
+        compiler_params=params(),
+        cost_estimate=cost(1e9, 1e6),
+        name="chain_state",
+    )(place, block_packs)
+    packs = lax.all_to_all(pack, "ep", split_axis=0, concat_axis=0, tiled=True)
     head_gain = subspace_gain_vector.reshape(1, -1)
-
-    def gated_part(part, first_slot):
-        ins = (head_gain, start, pack_a, pack_b, got, *packs)
-        return pl.pallas_call(
-            lambda *r: gated_kernel(heads, tp_count, first_slot, *r),
-            grid_spec=pltpu.PrefetchScalarGridSpec(
-                num_scalar_prefetch=1,
-                grid=(2,),
-                in_specs=[
-                    by_slot(rows, value_width),
-                    by_slot(rows, key_width),
-                    by_slot(rows, value_width),
-                ]
-                + [whole(a) for a in ins],
-                out_specs=[pl.BlockSpec((rows, value_width), lambda i, p: (0, 0))] * 2,
-                scratch_shapes=[pltpu.VMEM((tp_count, value_width, key_width), bf16)],
-            ),
-            out_shape=[jax.ShapeDtypeStruct((rows, value_width), bf16)] * 2,
-            compiler_params=params(),
-            cost_estimate=cost(2e9, 6e6),
-        )(place, *part, *ins)
-
-    gated_b = gated_part(part_b, 2)
-    gated_a = gated_part(part_a, 0)
-    gated = [*gated_a, *gated_b]
+    by_turn = lambda r, w: pl.BlockSpec(
+        (1, r, w), lambda i, p: (jnp.bitwise_xor(i, tp_count // 2), 0, 0)
+    )
+    ins = (head_gain, starting_memory, block_packs, packs)
+    gated = pl.pallas_call(
+        lambda *r: gated_kernel(heads, tp_count, *r),
+        grid_spec=pltpu.PrefetchScalarGridSpec(
+            num_scalar_prefetch=1,
+            grid=(tp_count,),
+            in_specs=[by_turn(*a.shape[1:]) for a in local] + [whole(a) for a in ins],
+            out_specs=[pl.BlockSpec((rows, value_width), lambda i, p: (0, 0))] * tp_count,
+            scratch_shapes=[pltpu.VMEM((tp_count, value_width, key_width), bf16)],
+        ),
+        out_shape=[jax.ShapeDtypeStruct((rows, value_width), bf16)] * tp_count,
+        compiler_params=params(),
+        cost_estimate=cost(2e9, 6e6),
+        name="gated_heads",
+    )(place, *local, *ins)
     per_token = [gated[0]] + [
         lax.ppermute(gated[n], "tp", [(t, t ^ n) for t in range(tp_count)])
         for n in range(1, tp_count)
     ]
 
     near_x = lax.ppermute(near_in, "tp", across)
-    shared_mine, shared_other = ffn([normed, normed_x], joint_weights, None, 1)
+    shared_mine, shared_other = ffn([normed, normed_x], joint_weights, None)
     shared_back = lax.ppermute(shared_other, "tp", across)
-    near_mine, near_other = ffn([near_in, near_x], expert_weights, 0, 2)
+    near_mine, near_other = ffn([near_in, near_x], expert_weights, 0)
     near_back = lax.ppermute(near_other, "tp", across)
     near_sum = pl.pallas_call(
-        sum_kernel,
-        in_specs=vmem(2),
+        lambda *r: sum_swap_kernel(slots, *r),
+        in_specs=smem + vmem(2),
         out_specs=vmem(ep_count),
         out_shape=[piece] * ep_count,
         compiler_params=params(),
         cost_estimate=cost(1e9, 3e6),
         name="near_sum",
-    )(near_mine, near_back)
+    )(ep_place, near_mine, near_back)
     near_ret = swap(near_sum)
-    far_mine, far_other = ffn([far_in], expert_weights, 1, 2, slots)
+    far_mine, far_other = ffn([far_in], expert_weights, 1, slots)
     far_back = lax.ppermute(far_other, "tp", across)
     far_sum = pl.pallas_call(
         sum_kernel,
@@ -691,22 +627,34 @@
         8 * tokens * near * feature_width,
     )
 
-    columns = 4
     out_width = result_matrix.shape[1]
-    mixer_sublayer_result = pl.pallas_call(
-        lambda *r: project_kernel(tp_count, *r),
-        grid=(columns,),
-        in_specs=smem
-        + [pl.BlockSpec((rows, value_width), lambda i: (0, 0))] * tp_count
-        + [
-            pl.BlockSpec((result_matrix.shape[0], out_width // columns), lambda i: (0, i)),
-        ],
-        out_specs=pl.BlockSpec((rows, out_width // columns), lambda i: (0, i)),
-        out_shape=jax.ShapeDtypeStruct((rows, out_width), bf16),
-        compiler_params=params(),
-        cost_estimate=cost(2 * rows * out_width * result_matrix.shape[0], 1e7),
-        name="result_project",
-    )(tp_place, *per_token, result_matrix)
+    columns = out_width // 2
+
+    def project(first, kind, before=()):
+        weight_specs = [
+            pl.BlockSpec(
+                (value_width, columns), lambda i, p, n=n: (jnp.bitwise_xor(p[1], n), i)
+            )
+            for n in (first, first + 1)
+        ]
+        out_spec = pl.BlockSpec((rows, columns), lambda i, p: (0, i))
+        return pl.pallas_call(
+            project_kernel,
+            grid_spec=pltpu.PrefetchScalarGridSpec(
+                num_scalar_prefetch=1,
+                grid=(2,),
+                in_specs=[pl.BlockSpec((rows, value_width), lambda i, p: (0, 0))] * 2
+                + weight_specs
+                + [out_spec] * len(before),
+                out_specs=out_spec,
+            ),
+            out_shape=jax.ShapeDtypeStruct((rows, out_width), kind),
+            compiler_params=params(),
+            cost_estimate=cost(rows * out_width * result_matrix.shape[0], 5e6),
+        )(place, *per_token[first : first + 2], result_matrix, result_matrix, *before)
+
+    partial = project(0, f32)
+    mixer_sublayer_result = project(2, bf16, (partial,))
     return (mixer_sublayer_result, moe_out)
 
 

time: 220 us -> 200 us (0.909)
  starting transfers between devices: 64.2 us -> 49.9 us
  local copies, waits for them, and re-layouts: 6.18 us -> 2.65 us
  Pallas kernels: 81 us -> 78 us
    ppermute x14 -> x7, waiting for transfers between devices: 42.9 us -> 0.02 us  [swap(): lax.ppermute(pieces[n], 'ep', [(e, e ^ n) for e in range(ep_count)])]
    ppermute x1, waiting for transfers between devices: 7.67 us -> 31.9 us  [body(): picks_x = lax.ppermute(picks, 'tp', across)]
    ppermute x1, waiting for transfers between devices: 5.74 us -> 18.6 us  [body(): far_back = lax.ppermute(far_other, 'tp', across)]
    ppermute x4 -> x0, starting transfers between devices: 11.5 us -> none  [the longest x3 9.45 us: body(): lax.ppermute(pair, 'ep', [(e, e + 2 * s) for e in range(ep_count - 2 * s)])]
    ppermute x14 -> x7, starting transfers between devices: 26.4 us -> 15.5 us  [swap(): lax.ppermute(pieces[n], 'ep', [(e, e ^ n) for e in range(ep_count)])]
    all_to_all x2 -> x3, starting transfers between devices: 12.1 us -> 19.2 us  [exchange(): out = lax.all_to_all(cut, 'ep', split_axis=0, concat_axis=0, tiled=True)]
    ppermute x1, waiting for transfers between devices: 0.01 us -> 5.52 us  [body(): near_x = lax.ppermute(near_in, 'tp', across)]
    ppermute x1, waiting for transfers between devices: 0.01 us -> 5.41 us  [body(): near_back = lax.ppermute(near_other, 'tp', across)]
  transfers between devices with their start and end apart: 39 -> 30, of which waited for: 14 -> 6; matrix products, arithmetic and copies ran while one was open for 1% -> 0% of each run, Pallas kernels for 34% -> 37%
where the time goes in v1:
time: 200 us; the launch traced here: 199 us
  Pallas kernels  78 us (39%)
  waiting for transfers between devices  66.7 us (33%)
  starting transfers between devices  49.9 us (25%)
  local copies, waits for them, and re-layouts  2.65 us (1%)
    ppermute x1, waiting for transfers between devices, body(): picks_x = lax.ppermute(picks, 'tp', across)  31.9 us
    pallas_call x2, Pallas kernels, local_part(): pl.pallas_call(lambda *r: local_kernel(heads, len(carried), *r), grid_spe...  27.4 us
    all_to_all x3, starting transfers between devices, exchange(): out = lax.all_to_all(cut, 'ep', split_axis=0, concat_axis=0, tiled=True)  19.2 us
    pallas_call x3, Pallas kernels, ffn(): pl.pallas_call(lambda *refs: ffn_kernel(arrays, held, slots, *refs), grid...  19.1 us
    ppermute x1, waiting for transfers between devices, body(): far_back = lax.ppermute(far_other, 'tp', across)  18.6 us
    ppermute x7, starting transfers between devices, swap(): lax.ppermute(pieces[n], 'ep', [(e, e ^ n) for e in range(ep_count)])  15.5 us
    pallas_call x2, Pallas kernels, project(): pl.pallas_call(project_kernel, grid_spec=pltpu.PrefetchScalarGridSpec(num...  10.2 us
    pallas_call x1, Pallas kernels, body(): pl.pallas_call(lambda *r: gated_kernel(heads, tp_count, *r), grid_spec=pl...  6.39 us
  transfers between devices with their start and end apart: 30, of which 6 were waited for; matrix products, arithmetic and copies ran while one was open for 0% of the time, Pallas kernels for 37%

profile of v1, /device:TPU:0, one launch (start us, length us, event | category | flops | bytes accessed | tf_op | source)
XLA Modules:
  0.0 198.7 jit_solution(12093717403650530272)
XLA Ops:
  0.7 2.6 %pack_own.1 = (bf16[128,2048]{1,0:T(8,128)(2,1)}, f32[192,128]{1,0:T(8,128)}, bf16[192,2048]{1,0:T(8,128)(2,1)}) custom-call(s32[1]{0:T(128)} %bitcast.r_0_, bf16[128,2048]{1,0:T(8,128)(2,1)} %r_1_.3, f32[1,2048]{1,0:T(1,128)} %bitcast.23, s32[2,128]{1,0:T(2,128)} %bitcast.28, f32[2,128]{1,0:T(2,128)} %bitcast.31), custom_call_target="tpu_custom_call" | custom-call | flops 2000000000 | bytes 4000000 | tf_op jit(solution)/shard_map/pack_own/pallas_call | solution.py:462
  3.3 7.3 %all-to-all-start.3 = ((bf16[8,24,2048]{2,1,0:T(8,128)(2,1)}), bf16[8,24,2048]{2,1,0:T(8,128)(2,1)S(1)}, u32[]{:S(2)}, u32[]{:S(2)}) async-start(bf16[8,24,2048]{2,1,0:T(8,128)(2,1)} %bitcast.20), calls=%async_computation.3 | async-start | bytes 1572864 | tf_op jit(solution)/shard_map/all_to_all | solution.py:485
  10.6 1.6 collective-permute-start.6
  12.7 1.5 collective-permute-start.7
  14.8 31.9 %collective-permute-done.7.r_5_ = s32[2,128]{1,0:T(2,128)S(1)} collective-permute-done((s32[2,128]{1,0:T(2,128)S(1)}, s32[2,128]{1,0:T(2,128)S(1)}, u32[]{:S(2)}, u32[]{:S(2)}) %collective-permute-start.7) | collective-permute-done | bytes 1056 | tf_op jit(solution)/shard_map/ppermute | solution.py:447
  47.5 3.3 %pack_both.1 = (bf16[128,2048]{1,0:T(8,128)(2,1)}, bf16[384,2048]{1,0:T(8,128)(2,1)}, f32[192,128]{1,0:T(8,128)}) custom-call(bf16[128,2048]{1,0:T(8,128)(2,1)} %get-tuple-element.47.r_0_.refs_0_, bf16[128,2048]{1,0:T(8,128)(2,1)} %copy-done.14, f32[1,2048]{1,0:T(1,128)} %bitcast.24, s32[2,128]{1,0:T(2,128)} %bitcast.29, f32[2,128]{1,0:T(2,128)} %bitcast.32, ...), custom_call_target="tpu_custom_call" | custom-call | flops 3000000000 | bytes 6000000 | tf_op jit(solution)/shard_map/pack_both/pallas_call | solution.py:490
  50.8 5.9 %all-to-all-start.1 = ((bf16[8,48,2048]{2,1,0:T(8,128)(2,1)}), bf16[8,48,2048]{2,1,0:T(8,128)(2,1)}, u32[]{:S(2)}, u32[]{:S(2)}) async-start(bf16[8,48,2048]{2,1,0:T(8,128)(2,1)} %bitcast.18), calls=%async_computation.1 | async-start | bytes 3145728 | tf_op jit(solution)/shard_map/all_to_all | solution.py:485
  58.4 13.7 %shard_map.221 = (f32[4,256,512]{2,1,0:T(8,128)}, bf16[4,256,256]{2,1,0:T(8,128)(2,1)}, bf16[4,256,512]{2,1,0:T(8,128)(2,1)}, f32[4,144,256]{2,1,0:T(8,128)}) custom-call(s32[2]{0:T(128)} %pad_add_fusion.r_0_.place_ref, bf16[256,2048]{1,0:T(8,128)(2,1)} %r_1_.2, bf16[256,2048]{1,0:T(8,128)(2,1)} %collective-permute-done.2.r_2_, f32[1,2048]{1,0:T(1,128)} %bitcast.25, ...), custom_call_target="tpu_custom_call" | custom-call | flops 10000000000 | bytes 10000000 | tf_op jit(solution)/shard_map/pallas_call | solution.py:537
  72.1 13.8 %shard_map.222 = (f32[4,256,512]{2,1,0:T(8,128)}, bf16[4,256,256]{2,1,0:T(8,128)(2,1)}, bf16[4,256,512]{2,1,0:T(8,128)(2,1)}, f32[4,144,256]{2,1,0:T(8,128)}) custom-call(s32[2]{0:T(128)} %pad_add_fusion.r_0_.place_ref, bf16[256,2048]{1,0:T(8,128)(2,1)} %collective-permute-done.r_1_, ...), custom_call_target="tpu_custom_call", output_to_operand_aliasing={{0}: (11, {}), {1}: (12, {}), {2}: (13, {}), {3}: (14, {})} | custom-call | flops 10000000000 | bytes 10000000 | tf_op jit(solution)/shard_map/pallas_call | solution.py:537
  85.9 2.0 chain_state.1
  87.9 4.8 %all-to-all-done.1 = bf16[8,48,2048]{2,1,0:T(8,128)(2,1)} async-done(((bf16[8,48,2048]{2,1,0:T(8,128)(2,1)}), bf16[8,48,2048]{2,1,0:T(8,128)(2,1)}, u32[]{:S(2)}, u32[]{:S(2)}) %all-to-all-start.1) | async-done | bytes 1572896 | tf_op jit(solution)/shard_map/all_to_all | solution.py:485
  92.6 3.5 %all-to-all-start = ((bf16[8,144,256]{2,1,0:T(8,128)(2,1)}), bf16[8,144,256]{2,1,0:T(8,128)(2,1)S(1)}, u32[]{:S(2)}, u32[]{:S(2)}) async-start(bf16[8,144,256]{2,1,0:T(8,128)(2,1)} %chain_state.1), calls=%async_computation | async-start | bytes 1179648 | tf_op jit(solution)/shard_map/all_to_all | solution.py:569
  96.2 7.0 %shard_map.226 = (bf16[192,2048]{1,0:T(8,128)(2,1)}, bf16[192,2048]{1,0:T(8,128)(2,1)}) custom-call(bf16[384,2048]{1,0:T(8,128)(2,1)} %bitcast.10.refs_0_, bf16[2,2048,256]{2,1,0:T(8,128)(2,1)} %refs_2_.5, bf16[2,2048,256]{2,1,0:T(8,128)(2,1)} %refs_3_.5, bf16[2,256,2048]{2,1,0:T(8,128)(2,1)} %refs_4_.3, ...), custom_call_target="tpu_custom_call" | custom-call | flops 2415919104 | bytes 9437184 | tf_op jit(solution)/shard_map/pallas_call | solution.py:173
  103.3 1.5 collective-permute-start.16
  105.3 18.6 %collective-permute-done.16.b_ref = bf16[192,2048]{1,0:T(8,128)(2,1)S(1)} collective-permute-done((bf16[192,2048]{1,0:T(8,128)(2,1)}, bf16[192,2048]{1,0:T(8,128)(2,1)S(1)}, u32[]{:S(2)}, u32[]{:S(2)}) %collective-permute-start.16) | collective-permute-done | bytes 786464 | tf_op jit(solution)/shard_map/ppermute | solution.py:610
  124.8 2.5 %far_sum.1 = bf16[192,2048]{1,0:T(8,128)(2,1)} custom-call(bf16[192,2048]{1,0:T(8,128)(2,1)} %get-tuple-element.53.a_ref, bf16[192,2048]{1,0:T(8,128)(2,1)} %copy-done.12), custom_call_target="tpu_custom_call" | custom-call | flops 1000000000 | bytes 3000000 | tf_op jit(solution)/shard_map/far_sum/pallas_call | solution.py:611
  127.3 5.9 %all-to-all-start.2 = ((bf16[8,24,2048]{2,1,0:T(8,128)(2,1)}), bf16[8,24,2048]{2,1,0:T(8,128)(2,1)S(1)}, u32[]{:S(2)}, u32[]{:S(2)}) async-start(bf16[8,24,2048]{2,1,0:T(8,128)(2,1)} %bitcast.19), calls=%async_computation.2 | async-start | bytes 1572864 | tf_op jit(solution)/shard_map/all_to_all | solution.py:485
  133.8 5.5 %collective-permute-done.17.refs_1_ = bf16[192,2048]{1,0:T(8,128)(2,1)S(1)} collective-permute-done((bf16[192,2048]{1,0:T(8,128)(2,1)S(1)}, bf16[192,2048]{1,0:T(8,128)(2,1)S(1)}, u32[]{:S(2)}, u32[]{:S(2)}) %collective-permute-start.17) | collective-permute-done | bytes 786464 | tf_op jit(solution)/shard_map/ppermute | solution.py:594
  140.2 7.0 %shard_map.227 = (bf16[192,2048]{1,0:T(8,128)(2,1)}, bf16[192,2048]{1,0:T(8,128)(2,1)}) custom-call(bf16[192,2048]{1,0:T(8,128)(2,1)} %bitcast.17, bf16[192,2048]{1,0:T(8,128)(2,1)} %copy-done.6, bf16[2,2048,256]{2,1,0:T(8,128)(2,1)} %refs_2_.5, bf16[2,2048,256]{2,1,0:T(8,128)(2,1)} %refs_3_.5, bf16[2,256,2048]{2,1,0:T(8,128)(2,1)} %refs_4_.3, ...), custom_call_target="tpu_custom_call" | custom-call | flops 2415919104 | bytes 9437184 | tf_op jit(solution)/shard_map/pallas_call | solution.py:173
  148.7 5.0 %shard_map.225 = (bf16[128,2048]{1,0:T(8,128)(2,1)}, bf16[128,2048]{1,0:T(8,128)(2,1)}) custom-call(bf16[128,2048]{1,0:T(8,128)(2,1)} %get-tuple-element.47.r_0_.refs_0_, bf16[128,2048]{1,0:T(8,128)(2,1)} %get-tuple-element.49.refs_1_, bf16[2048,128]{1,0:T(8,128)(2,1)} %refs_2_.3, bf16[2048,128]{1,0:T(8,128)(2,1)} %refs_3_.3, bf16[128,2048]{1,0:T(8,128)(2,1)} %refs_4_.2, ...), custom_call_target="tpu_custom_call" | custom-call | flops 805306368 | bytes 5242880 | tf_op jit(solution)/shard_map/pallas_call | solution.py:173
  154.3 6.4 %gated_heads.1 = (bf16[256,512]{1,0:T(8,128)(2,1)}, bf16[256,512]{1,0:T(8,128)(2,1)}, bf16[256,512]{1,0:T(8,128)(2,1)}, bf16[256,512]{1,0:T(8,128)(2,1)}) custom-call(s32[2]{0:T(128)} %pad_add_fusion.r_0_.place_ref, f32[4,256,512]{2,1,0:T(8,128)} %get-tuple-element.38.r_1_, bf16[4,256,256]{2,1,0:T(8,128)(2,1)} %get-tuple-element.39.r_2_, ...), custom_call_target="tpu_custom_call" | custom-call | flops 2000000000 | bytes 6000000 | tf_op jit(solution)/shard_map/gated_heads/pallas_call | solution.py:575
  160.7 1.6 collective-permute-start.3
  162.5 5.4 %collective-permute-done.18.r_2_ = bf16[192,2048]{1,0:T(8,128)(2,1)} collective-permute-done((bf16[192,2048]{1,0:T(8,128)(2,1)}, bf16[192,2048]{1,0:T(8,128)(2,1)}, u32[]{:S(2)}, u32[]{:S(2)}) %collective-permute-start.18) | collective-permute-done | bytes 786464 | tf_op jit(solution)/shard_map/ppermute | solution.py:598
  168.0 2.6 %near_sum.1 = (bf16[24,2048]{1,0:T(8,128)(2,1)}, bf16[24,2048]{1,0:T(8,128)(2,1)}, bf16[24,2048]{1,0:T(8,128)(2,1)}, bf16[24,2048]{1,0:T(8,128)(2,1)}, bf16[24,2...) custom-call(s32[1]{0:T(128)} %bitcast.r_0_, ...), custom_call_target="tpu_custom_call" | custom-call | flops 1000000000 | bytes 3000000 | tf_op jit(solution)/shard_map/near_sum/pallas_call | solution.py:599
  170.6 1.7 collective-permute-start.19
  173.8 4.9 %shard_map.223.refs_2_ = f32[256,2048]{1,0:T(8,128)} custom-call(s32[2]{0:T(128)} %pad_add_fusion.r_0_.place_ref, bf16[256,512]{1,0:T(8,128)(2,1)} %get-tuple-element.44.first_ref, bf16[256,512]{1,0:T(8,128)(2,1)} %copy-done.11, bf16[2048,2048]{1,0:T(8,128)(2,1)} %refs_1_.4, bf16[2048,2048]{1,0:T(8,128)(2,1)} %refs_1_.4), custom_call_target="tpu_custom_call" | custom-call | flops 1073741824 | bytes 5000000 | tf_op jit(solution)/shard_map/pallas_call | solution.py:641
  179.1 2.6 %collective-permute-start.21 = (bf16[24,2048]{1,0:T(8,128)(2,1)}, bf16[24,2048]{1,0:T(8,128)(2,1)S(1)}, u32[]{:S(2)}, u32[]{:S(2)}) collective-permute-start(bf16[24,2048]{1,0:T(8,128)(2,1)} %get-tuple-element.61), channel_id=1, source_target_pairs={{0,12},{4,8},{8,4},{12,0},{16,28},{20,24},{24,20},{28,16},{1,13},{... | collective-permute-start | bytes 294920 | tf_op jit(solution)/shard_map/ppermute | solution.py:478
  181.7 2.4 %collective-permute-start.22 = (bf16[24,2048]{1,0:T(8,128)(2,1)}, bf16[24,2048]{1,0:T(8,128)(2,1)S(1)}, u32[]{:S(2)}, u32[]{:S(2)}) collective-permute-start(bf16[24,2048]{1,0:T(8,128)(2,1)} %get-tuple-element.62), channel_id=1, source_target_pairs={{0,16},{4,20},{8,24},{12,28},{16,0},{20,4},{24,8},{28,12},{1,17},{... | collective-permute-start | bytes 294920 | tf_op jit(solution)/shard_map/ppermute | solution.py:478
  184.7 3.5 %collective-permute-start.24 = (bf16[24,2048]{1,0:T(8,128)(2,1)S(1)}, bf16[24,2048]{1,0:T(8,128)(2,1)S(1)}, u32[]{:S(2)}, u32[]{:S(2)}) collective-permute-start(bf16[24,2048]{1,0:T(8,128)(2,1)S(1)} %copy-done.16), channel_id=1, source_target_pairs={{0,24},{4,28},{8,16},{12,20},{16,8},{20,12},{24,0},{28,4},{1,25},{... | collective-permute-start | bytes 294920 | tf_op jit(solution)/shard_map/ppermute | solution.py:478
  188.3 3.2 %collective-permute-start.25 = (bf16[24,2048]{1,0:T(8,128)(2,1)S(1)}, bf16[24,2048]{1,0:T(8,128)(2,1)S(1)}, u32[]{:S(2)}, u32[]{:S(2)}) collective-permute-start(bf16[24,2048]{1,0:T(8,128)(2,1)S(1)} %copy-done.15), channel_id=1, source_target_pairs={{0,28},{4,24},{8,20},{12,16},{16,12},{20,8},{24,4},{28,0},{1,29},{... | collective-permute-start | bytes 294920 | tf_op jit(solution)/shard_map/ppermute | solution.py:478
  191.5 5.2 %shard_map.224 = bf16[256,2048]{1,0:T(8,128)(2,1)} custom-call(s32[2]{0:T(128)} %pad_add_fusion.r_0_.place_ref, bf16[256,512]{1,0:T(8,128)(2,1)} %copy-done.9, bf16[256,512]{1,0:T(8,128)(2,1)} %copy-done.10, bf16[2048,2048]{1,0:T(8,128)(2,1)} %refs_1_.4, bf16[2048,2048]{1,0:T(8,128)(2,1)} %refs_1_.4, f32[256,2048]{1,0:T(8,128)} %shard_map.223.refs_2_), custom_call_target="tpu_custom_call" | custom-call | flops 1073741824 | bytes 5000000 | tf_op jit(solution)/shard_map/pallas_call | solution.py:641
  196.8 1.9 shard_map.228
  (85 shorter events, 11.4 us)
Async XLA Ops:
  3.3 47.5 %all-to-all-start.3 = ((bf16[8,24,2048]{2,1,0:T(8,128)(2,1)}), bf16[8,24,2048]{2,1,0:T(8,128)(2,1)S(1)}, u32[]{:S(2)}, u32[]{:S(2)}) async-start(bf16[8,24,2048]{2,1,0:T(8,128)(2,1)} %bitcast.20), calls=%async_computation.3 | async-start | bytes 1572864 | tf_op jit(solution)/shard_map/all_to_all | solution.py:485
  10.6 36.1 %collective-permute-start.6 = (bf16[128,2048]{1,0:T(8,128)(2,1)S(1)}, bf16[128,2048]{1,0:T(8,128)(2,1)S(1)}, u32[]{:S(2)}, u32[]{:S(2)}) collective-permute-start(bf16[128,2048]{1,0:T(8,128)(2,1)S(1)} %copy-done.13), channel_id=1, source_target_pairs={{0,2},{1,3},{2,0},{3,1},{4,6},{5,7},{6,4},{7,5},{8,10},{9,11},{10,... | collective-permute-start | bytes 1572872 | tf_op jit(solution)/shard_map/ppermute | solution.py:446
  12.2 45.2 %collective-permute-start = (bf16[256,2048]{1,0:T(8,128)(2,1)}, bf16[256,2048]{1,0:T(8,128)(2,1)}, u32[]{:S(2)}, u32[]{:S(2)}) collective-permute-start(bf16[256,2048]{1,0:T(8,128)(2,1)} %r_1_.2), channel_id=1, source_target_pairs={{0,2},{1,3},{2,0},{3,1},{4,6},{5,7},{6,4},{7,5},{8,10},{9,11},{10,... | collective-permute-start | bytes 3145736 | tf_op jit(solution)/shard_map/ppermute | solution.py:449
  12.7 34.0 %collective-permute-start.7 = (s32[2,128]{1,0:T(2,128)S(1)}, s32[2,128]{1,0:T(2,128)S(1)}, u32[]{:S(2)}, u32[]{:S(2)}) collective-permute-start(s32[2,128]{1,0:T(2,128)S(1)} %bitcast.30), channel_id=1, source_target_pairs={{0,2},{1,3},{2,0},{3,1},{4,6},{5,7},{6,4},{7,5},{8,10},{9,11},{10,... | collective-permute-start | bytes 3080 | tf_op jit(solution)/shard_map/ppermute | solution.py:447
  14.2 32.5 %collective-permute-start.8 = (f32[2,128]{1,0:T(2,128)S(1)}, f32[2,128]{1,0:T(2,128)S(1)}, u32[]{:S(2)}, u32[]{:S(2)}) collective-permute-start(f32[2,128]{1,0:T(2,128)S(1)} %bitcast.33), channel_id=1, source_target_pairs={{0,2},{1,3},{2,0},{3,1},{4,6},{5,7},{6,4},{7,5},{8,10},{9,11},{10,... | collective-permute-start | bytes 3080 | tf_op jit(solution)/shard_map/ppermute | solution.py:448
  14.8 43.7 %collective-permute-start.2 = (bf16[256,2048]{1,0:T(8,128)(2,1)}, bf16[256,2048]{1,0:T(8,128)(2,1)}, u32[]{:S(2)}, u32[]{:S(2)}) collective-permute-start(bf16[256,2048]{1,0:T(8,128)(2,1)} %r_1_.2), channel_id=1, source_target_pairs={{0,1},{1,0},{2,3},{3,2},{4,5},{5,4},{6,7},{7,6},{8,9},{9,8},{10,11... | collective-permute-start | bytes 3145736 | tf_op jit(solution)/shard_map/ppermute | solution.py:450
  50.8 54.0 %copy-start.5 = (bf16[8,24,2048]{2,1,0:T(8,128)(2,1)}, bf16[8,24,2048]{2,1,0:T(8,128)(2,1)S(1)}, u32[]{:S(2)}) copy-start(bf16[8,24,2048]{2,1,0:T(8,128)(2,1)S(1)} %all-to-all-done.3) | copy-start | bytes 2359300
  50.8 41.9 %all-to-all-start.1 = ((bf16[8,48,2048]{2,1,0:T(8,128)(2,1)}), bf16[8,48,2048]{2,1,0:T(8,128)(2,1)}, u32[]{:S(2)}, u32[]{:S(2)}) async-start(bf16[8,48,2048]{2,1,0:T(8,128)(2,1)} %bitcast.18), calls=%async_computation.1 | async-start | bytes 3145728 | tf_op jit(solution)/shard_map/all_to_all | solution.py:485
  56.7 39.5 %collective-permute-start.13 = (bf16[2,2048,256]{2,1,0:T(8,128)(2,1)S(1)}, bf16[2,2048,256]{2,1,0:T(8,128)(2,1)}, u32[]{:S(2)}, u32[]{:S(2)}) collective-permute-start(bf16[2,2048,256]{2,1,0:T(8,128)(2,1)S(1)} %copy-done.4), channel_id=1, source_target_pairs={{0,1},{1,0},{2,3},{3,2},{4,5},{5,4},{6,7},{7,6},{8,9},{9,8},{10,11... | collective-permute-start | bytes 6291464 | tf_op jit(solution)/shard_map/ppermute | solution.py:455
  56.8 39.4 %collective-permute-start.14 = (bf16[2,2048,256]{2,1,0:T(8,128)(2,1)}, bf16[2,2048,256]{2,1,0:T(8,128)(2,1)}, u32[]{:S(2)}, u32[]{:S(2)}) collective-permute-start(bf16[2,2048,256]{2,1,0:T(8,128)(2,1)} %refs_3_.5), channel_id=1, source_target_pairs={{0,1},{1,0},{2,3},{3,2},{4,5},{5,4},{6,7},{7,6},{8,9},{9,8},{10,11... | collective-permute-start | bytes 6291464 | tf_op jit(solution)/shard_map/ppermute | solution.py:455
  57.3 38.9 %collective-permute-start.15 = (bf16[2,256,2048]{2,1,0:T(8,128)(2,1)}, bf16[2,256,2048]{2,1,0:T(8,128)(2,1)}, u32[]{:S(2)}, u32[]{:S(2)}) collective-permute-start(bf16[2,256,2048]{2,1,0:T(8,128)(2,1)} %refs_4_.3), channel_id=1, source_target_pairs={{0,1},{1,0},{2,3},{3,2},{4,5},{5,4},{6,7},{7,6},{8,9},{9,8},{10,11... | collective-permute-start | bytes 6291464 | tf_op jit(solution)/shard_map/ppermute | solution.py:455
  57.4 14.7 %collective-permute-start.1 = (bf16[256,2048]{1,0:T(8,128)(2,1)}, bf16[256,2048]{1,0:T(8,128)(2,1)}, u32[]{:S(2)}, u32[]{:S(2)}) collective-permute-start(bf16[256,2048]{1,0:T(8,128)(2,1)} %collective-permute-done.r_1_), channel_id=1, source_target_pairs={{0,1},{1,0},{2,3},{3,2},{4,5},{5,4},{6,7},{7,6},{8,9},{9,8},{10,11... | collective-permute-start | bytes 3145736 | tf_op jit(solution)/shard_map/ppermute | solution.py:451
  92.6 34.7 %all-to-all-start = ((bf16[8,144,256]{2,1,0:T(8,128)(2,1)}), bf16[8,144,256]{2,1,0:T(8,128)(2,1)S(1)}, u32[]{:S(2)}, u32[]{:S(2)}) async-start(bf16[8,144,256]{2,1,0:T(8,128)(2,1)} %chain_state.1), calls=%async_computation | async-start | bytes 1179648 | tf_op jit(solution)/shard_map/all_to_all | solution.py:569
  103.3 20.6 %collective-permute-start.16 = (bf16[192,2048]{1,0:T(8,128)(2,1)}, bf16[192,2048]{1,0:T(8,128)(2,1)S(1)}, u32[]{:S(2)}, u32[]{:S(2)}) collective-permute-start(bf16[192,2048]{1,0:T(8,128)(2,1)} %get-tuple-element.54), channel_id=1, source_target_pairs={{0,2},{1,3},{2,0},{3,1},{4,6},{5,7},{6,4},{7,5},{8,10},{9,11},{10,... | collective-permute-start | bytes 2359304 | tf_op jit(solution)/shard_map/ppermute | solution.py:610
  104.8 34.6 %collective-permute-start.17 = (bf16[192,2048]{1,0:T(8,128)(2,1)S(1)}, bf16[192,2048]{1,0:T(8,128)(2,1)S(1)}, u32[]{:S(2)}, u32[]{:S(2)}) collective-permute-start(bf16[192,2048]{1,0:T(8,128)(2,1)S(1)} %bitcast.16), channel_id=1, source_target_pairs={{0,2},{1,3},{2,0},{3,1},{4,6},{5,7},{6,4},{7,5},{8,10},{9,11},{10,... | collective-permute-start | bytes 2359304 | tf_op jit(solution)/shard_map/ppermute | solution.py:594
  127.3 19.9 %copy-start.7 = (bf16[8,144,256]{2,1,0:T(8,128)(2,1)}, bf16[8,144,256]{2,1,0:T(8,128)(2,1)S(1)}, u32[]{:S(2)}) copy-start(bf16[8,144,256]{2,1,0:T(8,128)(2,1)S(1)} %all-to-all-done.r_7_) | copy-start | bytes 1769476
  127.3 69.5 %all-to-all-start.2 = ((bf16[8,24,2048]{2,1,0:T(8,128)(2,1)}), bf16[8,24,2048]{2,1,0:T(8,128)(2,1)S(1)}, u32[]{:S(2)}, u32[]{:S(2)}) async-start(bf16[8,24,2048]{2,1,0:T(8,128)(2,1)} %bitcast.19), calls=%async_computation.2 | async-start | bytes 1572864 | tf_op jit(solution)/shard_map/all_to_all | solution.py:485
  133.2 15.5 %collective-permute-start.10 = (bf16[2048,128]{1,0:T(8,128)(2,1)}, bf16[2048,128]{1,0:T(8,128)(2,1)}, u32[]{:S(2)}, u32[]{:S(2)}) collective-permute-start(bf16[2048,128]{1,0:T(8,128)(2,1)} %refs_3_.3), channel_id=1, source_target_pairs={{0,1},{1,0},{2,3},{3,2},{4,5},{5,4},{6,7},{7,6},{8,9},{9,8},{10,11... | collective-permute-start | bytes 1572872 | tf_op jit(solution)/shard_map/ppermute | solution.py:453
  133.2 15.5 %collective-permute-start.11 = (bf16[128,2048]{1,0:T(8,128)(2,1)}, bf16[128,2048]{1,0:T(8,128)(2,1)}, u32[]{:S(2)}, u32[]{:S(2)}) collective-permute-start(bf16[128,2048]{1,0:T(8,128)(2,1)} %refs_4_.2), channel_id=1, source_target_pairs={{0,1},{1,0},{2,3},{3,2},{4,5},{5,4},{6,7},{7,6},{8,9},{9,8},{10,11... | collective-permute-start | bytes 1572872 | tf_op jit(solution)/shard_map/ppermute | solution.py:453
  133.7 15.0 %collective-permute-start.9 = (bf16[2048,128]{1,0:T(8,128)(2,1)S(1)}, bf16[2048,128]{1,0:T(8,128)(2,1)}, u32[]{:S(2)}, u32[]{:S(2)}) collective-permute-start(bf16[2048,128]{1,0:T(8,128)(2,1)S(1)} %copy-done.8), channel_id=1, source_target_pairs={{0,1},{1,0},{2,3},{3,2},{4,5},{5,4},{6,7},{7,6},{8,9},{9,8},{10,11... | collective-permute-start | bytes 1572872 | tf_op jit(solution)/shard_map/ppermute | solution.py:453
  147.2 20.7 %collective-permute-start.18 = (bf16[192,2048]{1,0:T(8,128)(2,1)}, bf16[192,2048]{1,0:T(8,128)(2,1)}, u32[]{:S(2)}, u32[]{:S(2)}) collective-permute-start(bf16[192,2048]{1,0:T(8,128)(2,1)} %get-tuple-element.57), channel_id=1, source_target_pairs={{0,2},{1,3},{2,0},{3,1},{4,6},{5,7},{6,4},{7,5},{8,10},{9,11},{10,... | collective-permute-start | bytes 2359304 | tf_op jit(solution)/shard_map/ppermute | solution.py:598
  153.8 25.3 %collective-permute-start.12 = (bf16[128,2048]{1,0:T(8,128)(2,1)}, bf16[128,2048]{1,0:T(8,128)(2,1)S(1)}, u32[]{:S(2)}, u32[]{:S(2)}) collective-permute-start(bf16[128,2048]{1,0:T(8,128)(2,1)} %get-tuple-element.51), channel_id=1, source_target_pairs={{0,2},{1,3},{2,0},{3,1},{4,6},{5,7},{6,4},{7,5},{8,10},{9,11},{10,... | collective-permute-start | bytes 1572872 | tf_op jit(solution)/shard_map/ppermute | solution.py:596
  160.7 11.6 %collective-permute-start.5 = (bf16[256,512]{1,0:T(8,128)(2,1)}, bf16[256,512]{1,0:T(8,128)(2,1)S(1)}, u32[]{:S(2)}, u32[]{:S(2)}) collective-permute-start(bf16[256,512]{1,0:T(8,128)(2,1)} %get-tuple-element.45), channel_id=1, source_target_pairs={{0,1},{1,0},{2,3},{3,2},{4,5},{5,4},{6,7},{7,6},{8,9},{9,8},{10,11... | collective-permute-start | bytes 786440 | tf_op jit(solution)/shard_map/ppermute | solution.py:590
  160.7 24.0 %collective-permute-start.3 = (bf16[256,512]{1,0:T(8,128)(2,1)}, bf16[256,512]{1,0:T(8,128)(2,1)S(1)}, u32[]{:S(2)}, u32[]{:S(2)}) collective-permute-start(bf16[256,512]{1,0:T(8,128)(2,1)} %get-tuple-element.42), channel_id=1, source_target_pairs={{0,2},{1,3},{2,0},{3,1},{4,6},{5,7},{6,4},{7,5},{8,10},{9,11},{10,... | collective-permute-start | bytes 786440 | tf_op jit(solution)/shard_map/ppermute | solution.py:590
  162.3 26.0 %collective-permute-start.4 = (bf16[256,512]{1,0:T(8,128)(2,1)}, bf16[256,512]{1,0:T(8,128)(2,1)S(1)}, u32[]{:S(2)}, u32[]{:S(2)}) collective-permute-start(bf16[256,512]{1,0:T(8,128)(2,1)} %get-tuple-element.43), channel_id=1, source_target_pairs={{0,3},{1,2},{2,1},{3,0},{4,7},{5,6},{6,5},{7,4},{8,11},{9,10},{10,... | collective-permute-start | bytes 786440 | tf_op jit(solution)/shard_map/ppermute | solution.py:590
  170.6 11.2 %collective-permute-start.19 = (bf16[24,2048]{1,0:T(8,128)(2,1)}, bf16[24,2048]{1,0:T(8,128)(2,1)S(1)}, u32[]{:S(2)}, u32[]{:S(2)}) collective-permute-start(bf16[24,2048]{1,0:T(8,128)(2,1)} %get-tuple-element.59), channel_id=1, source_target_pairs={{0,4},{4,0},{8,12},{12,8},{16,20},{20,16},{24,28},{28,24},{1,5},{5... | collective-permute-start | bytes 294920 | tf_op jit(solution)/shard_map/ppermute | solution.py:478
  172.3 11.8 %collective-permute-start.20 = (bf16[24,2048]{1,0:T(8,128)(2,1)}, bf16[24,2048]{1,0:T(8,128)(2,1)S(1)}, u32[]{:S(2)}, u32[]{:S(2)}) collective-permute-start(bf16[24,2048]{1,0:T(8,128)(2,1)} %get-tuple-element.60), channel_id=1, source_target_pairs={{0,8},{4,12},{8,0},{12,4},{16,24},{20,28},{24,16},{28,20},{1,9},{5... | collective-permute-start | bytes 294920 | tf_op jit(solution)/shard_map/ppermute | solution.py:478
  179.1 17.6 %collective-permute-start.21 = (bf16[24,2048]{1,0:T(8,128)(2,1)}, bf16[24,2048]{1,0:T(8,128)(2,1)S(1)}, u32[]{:S(2)}, u32[]{:S(2)}) collective-permute-start(bf16[24,2048]{1,0:T(8,128)(2,1)} %get-tuple-element.61), channel_id=1, source_target_pairs={{0,12},{4,8},{8,4},{12,0},{16,28},{20,24},{24,20},{28,16},{1,13},{... | collective-permute-start | bytes 294920 | tf_op jit(solution)/shard_map/ppermute | solution.py:478
  181.7 15.0 %collective-permute-start.22 = (bf16[24,2048]{1,0:T(8,128)(2,1)}, bf16[24,2048]{1,0:T(8,128)(2,1)S(1)}, u32[]{:S(2)}, u32[]{:S(2)}) collective-permute-start(bf16[24,2048]{1,0:T(8,128)(2,1)} %get-tuple-element.62), channel_id=1, source_target_pairs={{0,16},{4,20},{8,24},{12,28},{16,0},{20,4},{24,8},{28,12},{1,17},{... | collective-permute-start | bytes 294920 | tf_op jit(solution)/shard_map/ppermute | solution.py:478
  184.1 12.6 %collective-permute-start.23 = (bf16[24,2048]{1,0:T(8,128)(2,1)}, bf16[24,2048]{1,0:T(8,128)(2,1)S(1)}, u32[]{:S(2)}, u32[]{:S(2)}) collective-permute-start(bf16[24,2048]{1,0:T(8,128)(2,1)} %get-tuple-element.63), channel_id=1, source_target_pairs={{0,20},{4,16},{8,28},{12,24},{16,4},{20,0},{24,12},{28,8},{1,21},{... | collective-permute-start | bytes 294920 | tf_op jit(solution)/shard_map/ppermute | solution.py:478
  184.7 12.0 %collective-permute-start.24 = (bf16[24,2048]{1,0:T(8,128)(2,1)S(1)}, bf16[24,2048]{1,0:T(8,128)(2,1)S(1)}, u32[]{:S(2)}, u32[]{:S(2)}) collective-permute-start(bf16[24,2048]{1,0:T(8,128)(2,1)S(1)} %copy-done.16), channel_id=1, source_target_pairs={{0,24},{4,28},{8,16},{12,20},{16,8},{20,12},{24,0},{28,4},{1,25},{... | collective-permute-start | bytes 294920 | tf_op jit(solution)/shard_map/ppermute | solution.py:478
  188.3 8.5 %collective-permute-start.25 = (bf16[24,2048]{1,0:T(8,128)(2,1)S(1)}, bf16[24,2048]{1,0:T(8,128)(2,1)S(1)}, u32[]{:S(2)}, u32[]{:S(2)}) collective-permute-start(bf16[24,2048]{1,0:T(8,128)(2,1)S(1)} %copy-done.15), channel_id=1, source_target_pairs={{0,28},{4,24},{8,20},{12,16},{16,12},{20,8},{24,4},{28,0},{1,29},{... | collective-permute-start | bytes 294920 | tf_op jit(solution)/shard_map/ppermute | solution.py:478
  (19 other events, 125.2 us)

commit v2 on v1

--- a/solution.py
+++ b/solution.py
@@ -132,20 +132,16 @@
             ]
 
 
-def ffn_kernel(arrays, expert, slots, *refs):
+def ffn_kernel(arrays, held, slots, *refs):
     ins = refs[:arrays]
-    weights = refs[arrays : arrays + 6]
+    weights = [w[held] if len(w.shape) == 3 else w[...] for w in refs[arrays : arrays + 6]]
     outs = refs[arrays + 6 :]
     height = ins[0].shape[0]
     rows = jnp.concatenate([r[...] for r in ins], axis=0)
-    total = None
-    for n in range(2):
-        gate_w, up_w, down_w = (
-            w[...] if len(w.shape) == 2 else w[expert] for w in weights[3 * n : 3 * n + 3]
-        )
-        hidden = (silu(dot(rows, gate_w)) * dot(rows, up_w)).astype(bf16)
-        part = dot(hidden, down_w)
-        total = part if total is None else total + part
+    gate = dot(rows, jnp.concatenate([weights[0], weights[3]], axis=1))
+    up = dot(rows, jnp.concatenate([weights[1], weights[4]], axis=1))
+    hidden = (silu(gate) * up).astype(bf16)
+    total = dot(hidden, jnp.concatenate([weights[2], weights[5]], axis=0))
     if len(outs) == arrays:
         for k in range(arrays):
             outs[k][...] = total[k * height : (k + 1) * height].astype(bf16)
@@ -156,20 +152,19 @@
             outs[k][n * slots : (n + 1) * slots] = piece
 
 
-def ffn(rows, weights, expert, slots=None, grant=None):
+def ffn(rows, weights, expert, slots=None, grant=None, whole=False):
     arrays = len(rows)
     count, width = rows[0].shape
     inner = weights[0].shape[-1]
     outs = 2
     out = jax.ShapeDtypeStruct((arrays * count // outs, width), bf16)
-    held = expert
-    if grant is None and expert is not None:
-        held = 0
+    held = 0
+    if expert is None or whole:
+        held, weight_specs = expert, vmem(6)
+    else:
         weight_specs = [
             pl.BlockSpec((1,) + w.shape[1:], lambda i: (expert, 0, 0)) for w in weights
         ]
-    else:
-        weight_specs = vmem(6)
     return pl.pallas_call(
         lambda *refs: ffn_kernel(arrays, held, slots, *refs),
         grid=(1,),
@@ -236,19 +231,32 @@
     gain_ref, shift_ref, fade_ref = refs[:3]
     weight_refs = refs[3:8]
     out_ref, qg_ref, gate_ref, pack_ref = refs[8 + carried : 12 + carried]
-    buffer, sems = refs[12 + carried :]
-    d_ref, k_ref, q_ref, v_ref, g_ref = weight_refs
+    buffer, *held_weights, sems, weight_sems = refs[12 + carried :]
+    d_ref, k_ref, q_ref, v_ref, g_ref = held_weights
     slot = pl.program_id(0)
     span = SPAN_LENGTH
     key_width = q_ref.shape[1]
     value_width = v_ref.shape[1]
+    fetches = [
+        pltpu.make_async_copy(weight_refs[n], held_weights[n], weight_sems.at[n])
+        for n in range(5)
+    ]
 
     @pl.when(slot == 0)
     def _():
-        for n, ref in enumerate((first_ref, second_ref)):
-            pltpu.make_async_copy(ref, buffer.at[n], sems.at[n]).start()
+        pltpu.make_async_copy(first_ref, buffer.at[0], sems.at[0]).start()
+        for fetch in fetches:
+            fetch.start()
+        pltpu.make_async_copy(second_ref, buffer.at[1], sems.at[1]).start()
+
+    def ready(*which):
+        @pl.when(slot == 0)
+        def _():
+            for n in which:
+                fetches[n].wait()
 
     pltpu.make_async_copy(first_ref, buffer.at[slot], sems.at[slot]).wait()
+    ready(0, 1, 2, 3, 4)
     normed = rms_rows(buffer[slot], gain_ref[...])
     rows = normed.shape[0]
     logits = dot(normed, d_ref[...]).astype(bf16).astype(f32) + shift_ref[...]
@@ -310,7 +318,7 @@
             axis=1,
         )
         outer = dot(qb, held.astype(bf16), ((1,), (1,)))
-        out_ref[0, at, :] = inner + outer
+        out_ref[0, at, :] = (inner + outer).astype(bf16)
         qg_ref[0, at, :] = (qf * jnp.exp(passed)).astype(bf16)
         added = dot(vb, key_end, ((0,), (0,)))
         held = held * jnp.exp(total) + jnp.where(own_block, added, 0.0)
@@ -328,10 +336,10 @@
     return held * pack[DV : DV + 1].astype(f32) + pack[0:DV].astype(f32)
 
 
-def chain_kernel(blocks, place_ref, packs_ref, out_ref):
+def chain_kernel(blocks, of_tp, place_ref, packs_ref, out_ref):
     held = None
     for n in range(blocks):
-        pack = packs_ref[jnp.bitwise_xor(place_ref[1], n)]
+        pack = packs_ref[jnp.bitwise_xor(of_tp(place_ref), n)]
         if held is None:
             held, fading = pack[0:DV], pack[DV : DV + 1]
         else:
@@ -346,6 +354,8 @@
 def gated_kernel(
     heads,
     blocks,
+    of_ep,
+    of_tp,
     place_ref,
     local_ref,
     qg_ref,
@@ -364,13 +374,13 @@
     def _():
         held = start_ref[...].T
         for n in range(pack_ref.shape[0]):
-            held = jnp.where(place_ref[0] > n, follow(held, pack_ref[n]), held)
+            held = jnp.where(of_ep(place_ref) > n, follow(held, pack_ref[n]), held)
         width_bits = MATCHER_WIDTH.bit_length() - 1
         lane_head = jnp.right_shift(
             lax.broadcasted_iota(jnp.int32, (DV, key_width), 1), width_bits
         )
         for n in range(blocks):
-            slot = jnp.bitwise_xor(place_ref[1], n)
+            slot = jnp.bitwise_xor(of_tp(place_ref), n)
             for h in range(heads):
                 entering[slot, h * DV : (h + 1) * DV, :] = jnp.where(
                     lane_head == h, held, 0.0
@@ -378,7 +388,7 @@
             held = follow(held, block_ref[slot])
 
     slot = jnp.bitwise_xor(pl.program_id(0), blocks // 2)
-    attended = local_ref[0] + dot(qg_ref[0], entering[slot], ((1,), (1,)))
+    attended = local_ref[0].astype(f32) + dot(qg_ref[0], entering[slot], ((1,), (1,)))
     parts = []
     for h in range(heads):
         at = slice(h * DV, (h + 1) * DV)
@@ -433,6 +443,10 @@
     beside = [(t, t ^ 1) for t in range(tp_count)]
     ep_place = lax.axis_index("ep").astype(jnp.int32).reshape(1)
     tp_place = lax.axis_index("tp").astype(jnp.int32).reshape(1)
+    place = ep_place * tp_count + tp_place
+    tp_bits = tp_count.bit_length() - 1
+    of_tp = lambda p: jnp.bitwise_and(p[0], tp_count - 1)
+    of_ep = lambda p: jnp.right_shift(p[0], tp_bits)
 
     tokens, feature_width = specialist_microbatch.shape
     top_count = picked_specialists.shape[1]
@@ -470,14 +484,15 @@
         ],
         compiler_params=params(),
         cost_estimate=cost(2e9, 4e6),
-        name="pack_own",
+        name="pa",
     )(ep_place, specialist_microbatch, moe_gain, picks, factors)
 
     def swap(pieces):
-        return [pieces[0]] + [
-            lax.ppermute(pieces[n], "ep", [(e, e ^ n) for e in range(ep_count)])
-            for n in range(1, ep_count)
-        ]
+        out = [pieces[0]]
+        for n in range(1, ep_count):
+            pairs = [(e, e ^ n) for e in range(ep_count)]
+            out.append(lax.ppermute(pieces[n], "ep", pairs))
+        return out
 
     def exchange(rows):
         shape = rows.shape
@@ -496,9 +511,9 @@
             jax.ShapeDtypeStruct((far, feature_width), bf16),
             jax.ShapeDtypeStruct((near, tokens), f32),
         ],
-        compiler_params=params(),
+        compiler_params=params(63),
         cost_estimate=cost(3e9, 6e6),
-        name="pack_both",
+        name="pb",
     )(
         normed,
         moe_raw_x,
@@ -515,7 +530,6 @@
     value_width = content_matrix.shape[1]
     heads = value_width // DV
     pack_rows = DV + 16
-    place = jnp.concatenate([ep_place, tp_place])
     whole = lambda a: pl.BlockSpec(a.shape, lambda i, *_: (0,) * len(a.shape))
     mix_gain = mixer_gain_vector.reshape(1, -1)
     shift = fading_shift_vector.reshape(1, -1)
@@ -525,11 +539,11 @@
 
     def local_part(raws, first_slot, carried=()):
         fade_spec = pl.BlockSpec(
-            (heads, rows), lambda i, p: (0, jnp.bitwise_xor(i + first_slot, p[1]))
+            (heads, rows), lambda i, p: (0, jnp.bitwise_xor(i + first_slot, of_tp(p)))
         )
         by_slot = lambda r, w: pl.BlockSpec((1, r, w), lambda i, p: (i + first_slot, 0, 0))
         shapes = [
-            jax.ShapeDtypeStruct((tp_count, rows, value_width), f32),
+            jax.ShapeDtypeStruct((tp_count, rows, value_width), bf16),
             jax.ShapeDtypeStruct((tp_count, rows, key_width), bf16),
             jax.ShapeDtypeStruct((tp_count, rows, value_width), bf16),
             jax.ShapeDtypeStruct((tp_count, pack_rows, key_width), f32),
@@ -541,12 +555,13 @@
                 grid=(2,),
                 in_specs=[any_space] * 2
                 + [whole(mix_gain), whole(shift), fade_spec]
-                + vmem(5)
-                + [any_space] * len(carried),
+                + [any_space] * (5 + len(carried)),
                 out_specs=[by_slot(*shape.shape[1:]) for shape in shapes],
                 scratch_shapes=[
                     pltpu.VMEM((2, rows, feature_width), bf16),
+                    *[pltpu.VMEM(w.shape, bf16) for w in weights],
                     pltpu.SemaphoreType.DMA((2,)),
+                    pltpu.SemaphoreType.DMA((5,)),
                 ],
             ),
             out_shape=shapes,
@@ -558,13 +573,13 @@
     local = local_part((mixer_microbatch, mix_raw_c), 0)
     *local, block_packs = local_part((mix_raw_x, mix_raw_xc), 2, local)
     pack = pl.pallas_call(
-        lambda *r: chain_kernel(tp_count, *r),
+        lambda *r: chain_kernel(tp_count, of_tp, *r),
         in_specs=smem + vmem(1),
         out_specs=pl.BlockSpec(memory_space=pltpu.VMEM),
         out_shape=jax.ShapeDtypeStruct((ep_count, pack_rows, key_width), bf16),
         compiler_params=params(),
         cost_estimate=cost(1e9, 1e6),
-        name="chain_state",
+        name="chain",
     )(place, block_packs)
     packs = lax.all_to_all(pack, "ep", split_axis=0, concat_axis=0, tiled=True)
     head_gain = subspace_gain_vector.reshape(1, -1)
@@ -573,7 +588,7 @@
     )
     ins = (head_gain, starting_memory, block_packs, packs)
     gated = pl.pallas_call(
-        lambda *r: gated_kernel(heads, tp_count, *r),
+        lambda *r: gated_kernel(heads, tp_count, of_ep, of_tp, *r),
         grid_spec=pltpu.PrefetchScalarGridSpec(
             num_scalar_prefetch=1,
             grid=(tp_count,),
@@ -584,7 +599,7 @@
         out_shape=[jax.ShapeDtypeStruct((rows, value_width), bf16)] * tp_count,
         compiler_params=params(),
         cost_estimate=cost(2e9, 6e6),
-        name="gated_heads",
+        name="gated",
     )(place, *local, *ins)
     per_token = [gated[0]] + [
         lax.ppermute(gated[n], "tp", [(t, t ^ n) for t in range(tp_count)])
@@ -592,7 +607,7 @@
     ]
 
     near_x = lax.ppermute(near_in, "tp", across)
-    shared_mine, shared_other = ffn([normed, normed_x], joint_weights, None)
+    shared_mine, shared_other = ffn([normed, normed_x], joint_weights, None, grant=16)
     shared_back = lax.ppermute(shared_other, "tp", across)
     near_mine, near_other = ffn([near_in, near_x], expert_weights, 0)
     near_back = lax.ppermute(near_other, "tp", across)
@@ -603,7 +618,7 @@
         out_shape=[piece] * ep_count,
         compiler_params=params(),
         cost_estimate=cost(1e9, 3e6),
-        name="near_sum",
+        name="nsum",
     )(ep_place, near_mine, near_back)
     near_ret = swap(near_sum)
     far_mine, far_other = ffn([far_in], expert_weights, 1, slots)
@@ -615,7 +630,7 @@
         out_shape=jax.ShapeDtypeStruct((near, feature_width), bf16),
         compiler_params=params(),
         cost_estimate=cost(1e9, 3e6),
-        name="far_sum",
+        name="fsum",
     )(far_mine, far_back)
     far_ret = exchange(far_sum)
     (moe_out,) = column_split(
@@ -633,7 +648,7 @@
     def project(first, kind, before=()):
         weight_specs = [
             pl.BlockSpec(
-                (value_width, columns), lambda i, p, n=n: (jnp.bitwise_xor(p[1], n), i)
+                (value_width, columns), lambda i, p, n=n: (jnp.bitwise_xor(of_tp(p), n), i)
             )
             for n in (first, first + 1)
         ]

time: 200 us -> 198 us (0.990)
  Pallas kernels: 78 us -> 72.2 us
  local copies, waits for them, and re-layouts: 2.65 us -> 6.47 us
    unnamed x42 -> x50, local copies, waits for them, and re-layouts: 2.65 us -> 6.47 us
  transfers between devices with their start and end apart: 30 -> 30, of which waited for: 6 -> 6; matrix products, arithmetic and copies ran while one was open for 0% -> 0% of each run, Pallas kernels for 37% -> 34%
where the time goes in v2:
time: 198 us; the launch traced here: 197 us
  Pallas kernels  72.2 us (36%)
  waiting for transfers between devices  67.9 us (34%)
  starting transfers between devices  49.8 us (25%)
  local copies, waits for them, and re-layouts  6.47 us (3%)
    ppermute x1, waiting for transfers between devices, body(): picks_x = lax.ppermute(picks, 'tp', across)  31.9 us
    pallas_call x2, Pallas kernels, local_part(): pl.pallas_call(lambda *r: local_kernel(heads, len(carried), *r), grid_spe...  25.5 us
    all_to_all x3, starting transfers between devices, exchange(): out = lax.all_to_all(cut, 'ep', split_axis=0, concat_axis=0, tiled=True)  19 us
    ppermute x1, waiting for transfers between devices, body(): far_back = lax.ppermute(far_other, 'tp', across)  18.6 us
    pallas_call x3, Pallas kernels, ffn(): pl.pallas_call(lambda *refs: ffn_kernel(arrays, held, slots, *refs), grid...  17.2 us
    ppermute x7, starting transfers between devices, swap(): out.append(lax.ppermute(pieces[n], 'ep', pairs))  15.5 us
    pallas_call x2, Pallas kernels, project(): pl.pallas_call(project_kernel, grid_spec=pltpu.PrefetchScalarGridSpec(num...  8.8 us
    unnamed x50, local copies, waits for them, and re-layouts  6.47 us
  transfers between devices with their start and end apart: 30, of which 6 were waited for; matrix products, arithmetic and copies ran while one was open for 0% of the time, Pallas kernels for 34%

profile of v2, /device:TPU:0, one launch (start us, length us, event | category | flops | bytes accessed | tf_op | source)
XLA Modules:
  0.0 197.2 jit_solution(6836048385971317990)
XLA Ops:
  0.7 2.6 %pa.1 = (bf16[128,2048]{1,0:T(8,128)(2,1)}, f32[192,128]{1,0:T(8,128)}, bf16[192,2048]{1,0:T(8,128)(2,1)}) custom-call(s32[1]{0:T(128)} %bitcast.r_0_, bf16[128,2048]{1,0:T(8,128)(2,1)} %r_1_.3, f32[1,2048]{1,0:T(1,128)} %bitcast.21, s32[2,128]{1,0:T(2,128)} %bitcast.26, f32[2,128]{1,0:T(2,128)} %bitcast.29), custom_call_target="tpu_custom_call" | custom-call | flops 2000000000 | bytes 4000000 | tf_op jit(solution)/shard_map/pa/pallas_call | solution.py:476
  3.3 7.3 %all-to-all-start.3 = ((bf16[8,24,2048]{2,1,0:T(8,128)(2,1)}), bf16[8,24,2048]{2,1,0:T(8,128)(2,1)}, u32[]{:S(2)}, u32[]{:S(2)}) async-start(bf16[8,24,2048]{2,1,0:T(8,128)(2,1)} %bitcast.18), calls=%async_computation.3 | async-start | bytes 1572864 | tf_op jit(solution)/shard_map/all_to_all | solution.py:500
  10.6 1.6 collective-permute-start.6
  12.7 1.5 collective-permute-start.7
  14.8 31.9 %collective-permute-done.7.r_5_ = s32[2,128]{1,0:T(2,128)S(1)} collective-permute-done((s32[2,128]{1,0:T(2,128)S(1)}, s32[2,128]{1,0:T(2,128)S(1)}, u32[]{:S(2)}, u32[]{:S(2)}) %collective-permute-start.7) | collective-permute-done | bytes 1056 | tf_op jit(solution)/shard_map/ppermute | solution.py:461
  47.5 3.3 %pb.1 = (bf16[128,2048]{1,0:T(8,128)(2,1)}, bf16[384,2048]{1,0:T(8,128)(2,1)}, f32[192,128]{1,0:T(8,128)}) custom-call(bf16[128,2048]{1,0:T(8,128)(2,1)} %get-tuple-element.47.r_0_.refs_0_, bf16[128,2048]{1,0:T(8,128)(2,1)} %copy-done.18, f32[1,2048]{1,0:T(1,128)} %bitcast.22, s32[2,128]{1,0:T(2,128)} %bitcast.27, f32[2,128]{1,0:T(2,128)} %bitcast.30, ...), custom_call_target="tpu_custom_call" | custom-call | flops 3000000000 | bytes 6000000 | tf_op jit(solution)/shard_map/pb/pallas_call | solution.py:505
  50.8 5.8 %all-to-all-start.1 = ((bf16[8,48,2048]{2,1,0:T(8,128)(2,1)}), bf16[8,48,2048]{2,1,0:T(8,128)(2,1)}, u32[]{:S(2)}, u32[]{:S(2)}) async-start(bf16[8,48,2048]{2,1,0:T(8,128)(2,1)} %bitcast.16), calls=%async_computation.1 | async-start | bytes 3145728 | tf_op jit(solution)/shard_map/all_to_all | solution.py:500
  57.7 12.8 %shard_map.221 = (bf16[4,256,512]{2,1,0:T(8,128)(2,1)}, bf16[4,256,256]{2,1,0:T(8,128)(2,1)}, bf16[4,256,512]{2,1,0:T(8,128)(2,1)}, f32[4,144,256]{2,1,0:T(8,128)}) custom-call(s32[1]{0:T(128)S(6)} %add.3.r_0_.place_ref, bf16[256,2048]{1,0:T(8,128)(2,1)} %r_1_.2, bf16[256,2048]{1,0:T(8,128)(2,1)} %collective-permute-done.2.r_2_, f32[1,2048]{1,0:T(1,128)} %bitcast.23, ...), custom_call_target="tpu_custom_call" | custom-call | flops 10000000000 | bytes 10000000 | tf_op jit(solution)/shard_map/pallas_call | solution.py:551
  71.5 12.7 %shard_map.222 = (bf16[4,256,512]{2,1,0:T(8,128)(2,1)}, bf16[4,256,256]{2,1,0:T(8,128)(2,1)}, bf16[4,256,512]{2,1,0:T(8,128)(2,1)}, f32[4,144,256]{2,1,0:T(8,128)}) custom-call(s32[1]{0:T(128)S(6)} %add.3.r_0_.place_ref, bf16[256,2048]{1,0:T(8,128)(2,1)} %collective-permute-done.r_1_, ...), custom_call_target="tpu_custom_call", output_to_operand_aliasing={{0}: (11, {}), {1}: (12, {}), {2}: (13, {}), {3}: (14, {})} | custom-call | flops 10000000000 | bytes 10000000 | tf_op jit(solution)/shard_map/pallas_call | solution.py:551
  84.2 2.0 chain.1
  86.2 6.4 %all-to-all-done.1 = bf16[8,48,2048]{2,1,0:T(8,128)(2,1)} async-done(((bf16[8,48,2048]{2,1,0:T(8,128)(2,1)}), bf16[8,48,2048]{2,1,0:T(8,128)(2,1)}, u32[]{:S(2)}, u32[]{:S(2)}) %all-to-all-start.1) | async-done | bytes 1572896 | tf_op jit(solution)/shard_map/all_to_all | solution.py:500
  92.6 3.5 %all-to-all-start = ((bf16[8,144,256]{2,1,0:T(8,128)(2,1)}), bf16[8,144,256]{2,1,0:T(8,128)(2,1)S(1)}, u32[]{:S(2)}, u32[]{:S(2)}) async-start(bf16[8,144,256]{2,1,0:T(8,128)(2,1)} %chain.1), calls=%async_computation | async-start | bytes 1179648 | tf_op jit(solution)/shard_map/all_to_all | solution.py:584
  96.1 7.0 %shard_map.226 = (bf16[192,2048]{1,0:T(8,128)(2,1)}, bf16[192,2048]{1,0:T(8,128)(2,1)}) custom-call(bf16[384,2048]{1,0:T(8,128)(2,1)} %bitcast.10.refs_0_, bf16[2,2048,256]{2,1,0:T(8,128)(2,1)} %refs_2_.5, bf16[2,2048,256]{2,1,0:T(8,128)(2,1)} %refs_3_.5, bf16[2,256,2048]{2,1,0:T(8,128)(2,1)} %refs_4_.3, ...), custom_call_target="tpu_custom_call" | custom-call | flops 2415919104 | bytes 9437184 | tf_op jit(solution)/shard_map/pallas_call | solution.py:168
  105.2 18.6 %collective-permute-done.16.b_ref = bf16[192,2048]{1,0:T(8,128)(2,1)S(1)} collective-permute-done((bf16[192,2048]{1,0:T(8,128)(2,1)}, bf16[192,2048]{1,0:T(8,128)(2,1)S(1)}, u32[]{:S(2)}, u32[]{:S(2)}) %collective-permute-start.16) | collective-permute-done | bytes 786464 | tf_op jit(solution)/shard_map/ppermute | solution.py:625
  124.8 2.5 %fsum.1 = bf16[192,2048]{1,0:T(8,128)(2,1)} custom-call(bf16[192,2048]{1,0:T(8,128)(2,1)} %get-tuple-element.53.a_ref, bf16[192,2048]{1,0:T(8,128)(2,1)} %copy-done.16), custom_call_target="tpu_custom_call" | custom-call | flops 1000000000 | bytes 3000000 | tf_op jit(solution)/shard_map/fsum/pallas_call | solution.py:626
  128.1 5.9 %all-to-all-start.2 = ((bf16[8,24,2048]{2,1,0:T(8,128)(2,1)}), bf16[8,24,2048]{2,1,0:T(8,128)(2,1)S(1)}, u32[]{:S(2)}, u32[]{:S(2)}) async-start(bf16[8,24,2048]{2,1,0:T(8,128)(2,1)} %bitcast.17), calls=%async_computation.2 | async-start | bytes 1572864 | tf_op jit(solution)/shard_map/all_to_all | solution.py:500
  134.7 4.6 %collective-permute-done.17.refs_1_ = bf16[192,2048]{1,0:T(8,128)(2,1)} collective-permute-done((bf16[192,2048]{1,0:T(8,128)(2,1)}, bf16[192,2048]{1,0:T(8,128)(2,1)}, u32[]{:S(2)}, u32[]{:S(2)}) %collective-permute-start.17) | collective-permute-done | bytes 786464 | tf_op jit(solution)/shard_map/ppermute | solution.py:609
  139.3 7.0 %shard_map.227 = (bf16[192,2048]{1,0:T(8,128)(2,1)}, bf16[192,2048]{1,0:T(8,128)(2,1)}) custom-call(bf16[192,2048]{1,0:T(8,128)(2,1)} %bitcast.14.refs_0_, bf16[192,2048]{1,0:T(8,128)(2,1)} %collective-permute-done.17.refs_1_, bf16[2,2048,256]{2,1,0:T(8,128)(2,1)} %refs_2_.5, bf16[2,2048,256]{2,1,0:T(8,128)(2,1)} %refs_3_.5, bf16[2,256,2048]{2,1,0:T(8,128)(2,1)} %refs_4_.3, ...), custom_call_target="tpu_custom_call" | custom-call | flops 2415919104 | bytes 9437184 | tf_op jit(solution)/shard_map/pallas_call | solution.py:168
  146.4 1.5 collective-permute-start.18
  150.8 3.1 %shard_map.225 = (bf16[128,2048]{1,0:T(8,128)(2,1)S(1)}, bf16[128,2048]{1,0:T(8,128)(2,1)}) custom-call(bf16[128,2048]{1,0:T(8,128)(2,1)S(1)} %copy-done.3, bf16[128,2048]{1,0:T(8,128)(2,1)S(1)} %copy-done.4, bf16[2048,128]{1,0:T(8,128)(2,1)S(1)} %copy-done, bf16[2048,128]{1,0:T(8,128)(2,1)S(1)} %copy-done.1, bf16[128,2048]{1,0:T(8,128)(2,1)S(1)} %copy-done.2, ...), custom_call_target="tpu_custom_call" | custom-call | flops 805306368 | bytes 5242880 | tf_op jit(solution)/shard_map/pallas_call | solution.py:168
  154.4 5.6 %gated.1 = (bf16[256,512]{1,0:T(8,128)(2,1)}, bf16[256,512]{1,0:T(8,128)(2,1)}, bf16[256,512]{1,0:T(8,128)(2,1)}, bf16[256,512]{1,0:T(8,128)(2,1)}) custom-call(s32[1]{0:T(128)S(6)} %add.3.r_0_.place_ref, bf16[4,256,512]{2,1,0:T(8,128)(2,1)} %get-tuple-element.38.r_1_, bf16[4,256,256]{2,1,0:T(8,128)(2,1)} %get-tuple-element.39.r_2_, ...), custom_call_target="tpu_custom_call" | custom-call | flops 2000000000 | bytes 6000000 | tf_op jit(solution)/shard_map/gated/pallas_call | solution.py:590
  160.0 1.6 collective-permute-start.3
  161.9 5.2 %collective-permute-done.18.r_2_ = bf16[192,2048]{1,0:T(8,128)(2,1)} collective-permute-done((bf16[192,2048]{1,0:T(8,128)(2,1)}, bf16[192,2048]{1,0:T(8,128)(2,1)}, u32[]{:S(2)}, u32[]{:S(2)}) %collective-permute-start.18) | collective-permute-done | bytes 786464 | tf_op jit(solution)/shard_map/ppermute | solution.py:613
  167.1 2.7 %nsum.1 = (bf16[24,2048]{1,0:T(8,128)(2,1)}, bf16[24,2048]{1,0:T(8,128)(2,1)}, bf16[24,2048]{1,0:T(8,128)(2,1)}, bf16[24,2048]{1,0:T(8,128)(2,1)}, bf16[24,2048]...) custom-call(s32[1]{0:T(128)} %bitcast.r_0_, ...), custom_call_target="tpu_custom_call" | custom-call | flops 1000000000 | bytes 3000000 | tf_op jit(solution)/shard_map/nsum/pallas_call | solution.py:614
  169.8 1.7 collective-permute-start.19
  173.0 4.2 %shard_map.223.refs_2_ = f32[256,2048]{1,0:T(8,128)} custom-call(s32[1]{0:T(128)S(6)} %add.3.r_0_.place_ref, bf16[256,512]{1,0:T(8,128)(2,1)} %get-tuple-element.44.first_ref, bf16[256,512]{1,0:T(8,128)(2,1)} %copy-done.14, bf16[2048,2048]{1,0:T(8,128)(2,1)} %refs_1_.4, bf16[2048,2048]{1,0:T(8,128)(2,1)} %refs_1_.4), custom_call_target="tpu_custom_call" | custom-call | flops 1073741824 | bytes 5000000 | tf_op jit(solution)/shard_map/pallas_call | solution.py:656
  178.2 2.6 %collective-permute-start.21 = (bf16[24,2048]{1,0:T(8,128)(2,1)}, bf16[24,2048]{1,0:T(8,128)(2,1)S(1)}, u32[]{:S(2)}, u32[]{:S(2)}) collective-permute-start(bf16[24,2048]{1,0:T(8,128)(2,1)} %get-tuple-element.61), channel_id=1, source_target_pairs={{0,12},{4,8},{8,4},{12,0},{16,28},{20,24},{24,20},{28,16},{1,13},{... | collective-permute-start | bytes 294920 | tf_op jit(solution)/shard_map/ppermute | solution.py:494
  180.9 2.4 %collective-permute-start.22 = (bf16[24,2048]{1,0:T(8,128)(2,1)}, bf16[24,2048]{1,0:T(8,128)(2,1)S(1)}, u32[]{:S(2)}, u32[]{:S(2)}) collective-permute-start(bf16[24,2048]{1,0:T(8,128)(2,1)} %get-tuple-element.62), channel_id=1, source_target_pairs={{0,16},{4,20},{8,24},{12,28},{16,0},{20,4},{24,8},{28,12},{1,17},{... | collective-permute-start | bytes 294920 | tf_op jit(solution)/shard_map/ppermute | solution.py:494
  183.9 3.6 %collective-permute-start.24 = (bf16[24,2048]{1,0:T(8,128)(2,1)S(1)}, bf16[24,2048]{1,0:T(8,128)(2,1)S(1)}, u32[]{:S(2)}, u32[]{:S(2)}) collective-permute-start(bf16[24,2048]{1,0:T(8,128)(2,1)S(1)} %copy-done.20), channel_id=1, source_target_pairs={{0,24},{4,28},{8,16},{12,20},{16,8},{20,12},{24,0},{28,4},{1,25},{... | collective-permute-start | bytes 294920 | tf_op jit(solution)/shard_map/ppermute | solution.py:494
  187.4 3.2 %collective-permute-start.25 = (bf16[24,2048]{1,0:T(8,128)(2,1)S(1)}, bf16[24,2048]{1,0:T(8,128)(2,1)S(1)}, u32[]{:S(2)}, u32[]{:S(2)}) collective-permute-start(bf16[24,2048]{1,0:T(8,128)(2,1)S(1)} %copy-done.19), channel_id=1, source_target_pairs={{0,28},{4,24},{8,20},{12,16},{16,12},{20,8},{24,4},{28,0},{1,29},{... | collective-permute-start | bytes 294920 | tf_op jit(solution)/shard_map/ppermute | solution.py:494
  190.6 4.6 %shard_map.224 = bf16[256,2048]{1,0:T(8,128)(2,1)} custom-call(s32[1]{0:T(128)S(6)} %add.3.r_0_.place_ref, bf16[256,512]{1,0:T(8,128)(2,1)} %copy-done.12, bf16[256,512]{1,0:T(8,128)(2,1)} %copy-done.13, bf16[2048,2048]{1,0:T(8,128)(2,1)} %refs_1_.4, bf16[2048,2048]{1,0:T(8,128)(2,1)} %refs_1_.4, f32[256,2048]{1,0:T(8,128)} %shard_map.223.refs_2_), custom_call_target="tpu_custom_call" | custom-call | flops 1073741824 | bytes 5000000 | tf_op jit(solution)/shard_map/pallas_call | solution.py:656
  195.3 1.9 shard_map.228
  (92 shorter events, 15.3 us)
Async XLA Ops:
  3.3 47.5 %all-to-all-start.3 = ((bf16[8,24,2048]{2,1,0:T(8,128)(2,1)}), bf16[8,24,2048]{2,1,0:T(8,128)(2,1)}, u32[]{:S(2)}, u32[]{:S(2)}) async-start(bf16[8,24,2048]{2,1,0:T(8,128)(2,1)} %bitcast.18), calls=%async_computation.3 | async-start | bytes 1572864 | tf_op jit(solution)/shard_map/all_to_all | solution.py:500
  10.6 36.1 %collective-permute-start.6 = (bf16[128,2048]{1,0:T(8,128)(2,1)S(1)}, bf16[128,2048]{1,0:T(8,128)(2,1)S(1)}, u32[]{:S(2)}, u32[]{:S(2)}) collective-permute-start(bf16[128,2048]{1,0:T(8,128)(2,1)S(1)} %copy-done.17), channel_id=1, source_target_pairs={{0,2},{1,3},{2,0},{3,1},{4,6},{5,7},{6,4},{7,5},{8,10},{9,11},{10,... | collective-permute-start | bytes 1572872 | tf_op jit(solution)/shard_map/ppermute | solution.py:460
  12.2 45.1 %collective-permute-start = (bf16[256,2048]{1,0:T(8,128)(2,1)}, bf16[256,2048]{1,0:T(8,128)(2,1)}, u32[]{:S(2)}, u32[]{:S(2)}) collective-permute-start(bf16[256,2048]{1,0:T(8,128)(2,1)} %r_1_.2), channel_id=1, source_target_pairs={{0,2},{1,3},{2,0},{3,1},{4,6},{5,7},{6,4},{7,5},{8,10},{9,11},{10,... | collective-permute-start | bytes 3145736 | tf_op jit(solution)/shard_map/ppermute | solution.py:463
  12.7 34.0 %collective-permute-start.7 = (s32[2,128]{1,0:T(2,128)S(1)}, s32[2,128]{1,0:T(2,128)S(1)}, u32[]{:S(2)}, u32[]{:S(2)}) collective-permute-start(s32[2,128]{1,0:T(2,128)S(1)} %bitcast.28), channel_id=1, source_target_pairs={{0,2},{1,3},{2,0},{3,1},{4,6},{5,7},{6,4},{7,5},{8,10},{9,11},{10,... | collective-permute-start | bytes 3080 | tf_op jit(solution)/shard_map/ppermute | solution.py:461
  14.2 32.5 %collective-permute-start.8 = (f32[2,128]{1,0:T(2,128)S(1)}, f32[2,128]{1,0:T(2,128)S(1)}, u32[]{:S(2)}, u32[]{:S(2)}) collective-permute-start(f32[2,128]{1,0:T(2,128)S(1)} %bitcast.31), channel_id=1, source_target_pairs={{0,2},{1,3},{2,0},{3,1},{4,6},{5,7},{6,4},{7,5},{8,10},{9,11},{10,... | collective-permute-start | bytes 3080 | tf_op jit(solution)/shard_map/ppermute | solution.py:462
  14.8 43.0 %collective-permute-start.2 = (bf16[256,2048]{1,0:T(8,128)(2,1)}, bf16[256,2048]{1,0:T(8,128)(2,1)}, u32[]{:S(2)}, u32[]{:S(2)}) collective-permute-start(bf16[256,2048]{1,0:T(8,128)(2,1)} %r_1_.2), channel_id=1, source_target_pairs={{0,1},{1,0},{2,3},{3,2},{4,5},{5,4},{6,7},{7,6},{8,9},{9,8},{10,11... | collective-permute-start | bytes 3145736 | tf_op jit(solution)/shard_map/ppermute | solution.py:464
  50.8 41.7 %all-to-all-start.1 = ((bf16[8,48,2048]{2,1,0:T(8,128)(2,1)}), bf16[8,48,2048]{2,1,0:T(8,128)(2,1)}, u32[]{:S(2)}, u32[]{:S(2)}) async-start(bf16[8,48,2048]{2,1,0:T(8,128)(2,1)} %bitcast.16), calls=%async_computation.1 | async-start | bytes 3145728 | tf_op jit(solution)/shard_map/all_to_all | solution.py:500
  56.6 39.5 %collective-permute-start.13 = (bf16[2,2048,256]{2,1,0:T(8,128)(2,1)S(1)}, bf16[2,2048,256]{2,1,0:T(8,128)(2,1)}, u32[]{:S(2)}, u32[]{:S(2)}) collective-permute-start(bf16[2,2048,256]{2,1,0:T(8,128)(2,1)S(1)} %copy-done.10), channel_id=1, source_target_pairs={{0,1},{1,0},{2,3},{3,2},{4,5},{5,4},{6,7},{7,6},{8,9},{9,8},{10,11... | collective-permute-start | bytes 6291464 | tf_op jit(solution)/shard_map/ppermute | solution.py:469
  56.7 39.4 %collective-permute-start.14 = (bf16[2,2048,256]{2,1,0:T(8,128)(2,1)}, bf16[2,2048,256]{2,1,0:T(8,128)(2,1)}, u32[]{:S(2)}, u32[]{:S(2)}) collective-permute-start(bf16[2,2048,256]{2,1,0:T(8,128)(2,1)} %refs_3_.5), channel_id=1, source_target_pairs={{0,1},{1,0},{2,3},{3,2},{4,5},{5,4},{6,7},{7,6},{8,9},{9,8},{10,11... | collective-permute-start | bytes 6291464 | tf_op jit(solution)/shard_map/ppermute | solution.py:469
  57.2 38.9 %collective-permute-start.15 = (bf16[2,256,2048]{2,1,0:T(8,128)(2,1)}, bf16[2,256,2048]{2,1,0:T(8,128)(2,1)}, u32[]{:S(2)}, u32[]{:S(2)}) collective-permute-start(bf16[2,256,2048]{2,1,0:T(8,128)(2,1)} %refs_4_.3), channel_id=1, source_target_pairs={{0,1},{1,0},{2,3},{3,2},{4,5},{5,4},{6,7},{7,6},{8,9},{9,8},{10,11... | collective-permute-start | bytes 6291464 | tf_op jit(solution)/shard_map/ppermute | solution.py:469
  57.3 13.2 %collective-permute-start.1 = (bf16[256,2048]{1,0:T(8,128)(2,1)}, bf16[256,2048]{1,0:T(8,128)(2,1)S(1)}, u32[]{:S(2)}, u32[]{:S(2)}) collective-permute-start(bf16[256,2048]{1,0:T(8,128)(2,1)} %collective-permute-done.r_1_), channel_id=1, source_target_pairs={{0,1},{1,0},{2,3},{3,2},{4,5},{5,4},{6,7},{7,6},{8,9},{9,8},{10,11... | collective-permute-start | bytes 3145736 | tf_op jit(solution)/shard_map/ppermute | solution.py:465
  92.6 34.7 %all-to-all-start = ((bf16[8,144,256]{2,1,0:T(8,128)(2,1)}), bf16[8,144,256]{2,1,0:T(8,128)(2,1)S(1)}, u32[]{:S(2)}, u32[]{:S(2)}) async-start(bf16[8,144,256]{2,1,0:T(8,128)(2,1)} %chain.1), calls=%async_computation | async-start | bytes 1179648 | tf_op jit(solution)/shard_map/all_to_all | solution.py:584
  103.2 20.6 %collective-permute-start.16 = (bf16[192,2048]{1,0:T(8,128)(2,1)}, bf16[192,2048]{1,0:T(8,128)(2,1)S(1)}, u32[]{:S(2)}, u32[]{:S(2)}) collective-permute-start(bf16[192,2048]{1,0:T(8,128)(2,1)} %get-tuple-element.54), channel_id=1, source_target_pairs={{0,2},{1,3},{2,0},{3,1},{4,6},{5,7},{6,4},{7,5},{8,10},{9,11},{10,... | collective-permute-start | bytes 2359304 | tf_op jit(solution)/shard_map/ppermute | solution.py:625
  104.7 34.7 %collective-permute-start.17 = (bf16[192,2048]{1,0:T(8,128)(2,1)}, bf16[192,2048]{1,0:T(8,128)(2,1)}, u32[]{:S(2)}, u32[]{:S(2)}) collective-permute-start(bf16[192,2048]{1,0:T(8,128)(2,1)} %bitcast.14.refs_0_), channel_id=1, source_target_pairs={{0,2},{1,3},{2,0},{3,1},{4,6},{5,7},{6,4},{7,5},{8,10},{9,11},{10,... | collective-permute-start | bytes 2359304 | tf_op jit(solution)/shard_map/ppermute | solution.py:609
  128.1 67.1 %all-to-all-start.2 = ((bf16[8,24,2048]{2,1,0:T(8,128)(2,1)}), bf16[8,24,2048]{2,1,0:T(8,128)(2,1)S(1)}, u32[]{:S(2)}, u32[]{:S(2)}) async-start(bf16[8,24,2048]{2,1,0:T(8,128)(2,1)} %bitcast.17), calls=%async_computation.2 | async-start | bytes 1572864 | tf_op jit(solution)/shard_map/all_to_all | solution.py:500
  134.0 14.7 %copy-start.3 = (bf16[128,2048]{1,0:T(8,128)(2,1)S(1)}, bf16[128,2048]{1,0:T(8,128)(2,1)}, u32[]{:S(2)}) copy-start(bf16[128,2048]{1,0:T(8,128)(2,1)} %get-tuple-element.47.r_0_.refs_0_) | copy-start | bytes 1572868
  134.1 13.8 %collective-permute-start.10 = (bf16[2048,128]{1,0:T(8,128)(2,1)S(1)}, bf16[2048,128]{1,0:T(8,128)(2,1)S(1)}, u32[]{:S(2)}, u32[]{:S(2)}) collective-permute-start(bf16[2048,128]{1,0:T(8,128)(2,1)S(1)} %copy-done.1), channel_id=1, source_target_pairs={{0,1},{1,0},{2,3},{3,2},{4,5},{5,4},{6,7},{7,6},{8,9},{9,8},{10,11... | collective-permute-start | bytes 1572872 | tf_op jit(solution)/shard_map/ppermute | solution.py:467
  134.1 14.6 %collective-permute-start.11 = (bf16[128,2048]{1,0:T(8,128)(2,1)S(1)}, bf16[128,2048]{1,0:T(8,128)(2,1)}, u32[]{:S(2)}, u32[]{:S(2)}) collective-permute-start(bf16[128,2048]{1,0:T(8,128)(2,1)S(1)} %copy-done.2), channel_id=1, source_target_pairs={{0,1},{1,0},{2,3},{3,2},{4,5},{5,4},{6,7},{7,6},{8,9},{9,8},{10,11... | collective-permute-start | bytes 1572872 | tf_op jit(solution)/shard_map/ppermute | solution.py:467
  134.6 14.1 %collective-permute-start.9 = (bf16[2048,128]{1,0:T(8,128)(2,1)S(1)}, bf16[2048,128]{1,0:T(8,128)(2,1)}, u32[]{:S(2)}, u32[]{:S(2)}) collective-permute-start(bf16[2048,128]{1,0:T(8,128)(2,1)S(1)} %copy-done), channel_id=1, source_target_pairs={{0,1},{1,0},{2,3},{3,2},{4,5},{5,4},{6,7},{7,6},{8,9},{9,8},{10,11... | collective-permute-start | bytes 1572872 | tf_op jit(solution)/shard_map/ppermute | solution.py:467
  146.4 20.7 %collective-permute-start.18 = (bf16[192,2048]{1,0:T(8,128)(2,1)}, bf16[192,2048]{1,0:T(8,128)(2,1)}, u32[]{:S(2)}, u32[]{:S(2)}) collective-permute-start(bf16[192,2048]{1,0:T(8,128)(2,1)} %get-tuple-element.57), channel_id=1, source_target_pairs={{0,2},{1,3},{2,0},{3,1},{4,6},{5,7},{6,4},{7,5},{8,10},{9,11},{10,... | collective-permute-start | bytes 2359304 | tf_op jit(solution)/shard_map/ppermute | solution.py:613
  153.9 24.4 %collective-permute-start.12 = (bf16[128,2048]{1,0:T(8,128)(2,1)}, bf16[128,2048]{1,0:T(8,128)(2,1)S(1)}, u32[]{:S(2)}, u32[]{:S(2)}) collective-permute-start(bf16[128,2048]{1,0:T(8,128)(2,1)} %get-tuple-element.51), channel_id=1, source_target_pairs={{0,2},{1,3},{2,0},{3,1},{4,6},{5,7},{6,4},{7,5},{8,10},{9,11},{10,... | collective-permute-start | bytes 1572872 | tf_op jit(solution)/shard_map/ppermute | solution.py:611
  160.0 11.5 %collective-permute-start.5 = (bf16[256,512]{1,0:T(8,128)(2,1)}, bf16[256,512]{1,0:T(8,128)(2,1)S(1)}, u32[]{:S(2)}, u32[]{:S(2)}) collective-permute-start(bf16[256,512]{1,0:T(8,128)(2,1)} %get-tuple-element.45), channel_id=1, source_target_pairs={{0,1},{1,0},{2,3},{3,2},{4,5},{5,4},{6,7},{7,6},{8,9},{9,8},{10,11... | collective-permute-start | bytes 786440 | tf_op jit(solution)/shard_map/ppermute | solution.py:605
  160.0 23.9 %collective-permute-start.3 = (bf16[256,512]{1,0:T(8,128)(2,1)}, bf16[256,512]{1,0:T(8,128)(2,1)S(1)}, u32[]{:S(2)}, u32[]{:S(2)}) collective-permute-start(bf16[256,512]{1,0:T(8,128)(2,1)} %get-tuple-element.42), channel_id=1, source_target_pairs={{0,2},{1,3},{2,0},{3,1},{4,6},{5,7},{6,4},{7,5},{8,10},{9,11},{10,... | collective-permute-start | bytes 786440 | tf_op jit(solution)/shard_map/ppermute | solution.py:605
  161.6 25.9 %collective-permute-start.4 = (bf16[256,512]{1,0:T(8,128)(2,1)}, bf16[256,512]{1,0:T(8,128)(2,1)S(1)}, u32[]{:S(2)}, u32[]{:S(2)}) collective-permute-start(bf16[256,512]{1,0:T(8,128)(2,1)} %get-tuple-element.43), channel_id=1, source_target_pairs={{0,3},{1,2},{2,1},{3,0},{4,7},{5,6},{6,5},{7,4},{8,11},{9,10},{10,... | collective-permute-start | bytes 786440 | tf_op jit(solution)/shard_map/ppermute | solution.py:605
  169.8 11.1 %collective-permute-start.19 = (bf16[24,2048]{1,0:T(8,128)(2,1)}, bf16[24,2048]{1,0:T(8,128)(2,1)S(1)}, u32[]{:S(2)}, u32[]{:S(2)}) collective-permute-start(bf16[24,2048]{1,0:T(8,128)(2,1)} %get-tuple-element.59), channel_id=1, source_target_pairs={{0,4},{4,0},{8,12},{12,8},{16,20},{20,16},{24,28},{28,24},{1,5},{5... | collective-permute-start | bytes 294920 | tf_op jit(solution)/shard_map/ppermute | solution.py:494
  171.5 11.7 %collective-permute-start.20 = (bf16[24,2048]{1,0:T(8,128)(2,1)}, bf16[24,2048]{1,0:T(8,128)(2,1)S(1)}, u32[]{:S(2)}, u32[]{:S(2)}) collective-permute-start(bf16[24,2048]{1,0:T(8,128)(2,1)} %get-tuple-element.60), channel_id=1, source_target_pairs={{0,8},{4,12},{8,0},{12,4},{16,24},{20,28},{24,16},{28,20},{1,9},{5... | collective-permute-start | bytes 294920 | tf_op jit(solution)/shard_map/ppermute | solution.py:494
  173.0 14.4 %copy-start.19 = (bf16[24,2048]{1,0:T(8,128)(2,1)S(1)}, bf16[24,2048]{1,0:T(8,128)(2,1)}, u32[]{:S(2)}) copy-start(bf16[24,2048]{1,0:T(8,128)(2,1)} %get-tuple-element.65) | copy-start | bytes 294916
  178.2 17.0 %collective-permute-start.21 = (bf16[24,2048]{1,0:T(8,128)(2,1)}, bf16[24,2048]{1,0:T(8,128)(2,1)S(1)}, u32[]{:S(2)}, u32[]{:S(2)}) collective-permute-start(bf16[24,2048]{1,0:T(8,128)(2,1)} %get-tuple-element.61), channel_id=1, source_target_pairs={{0,12},{4,8},{8,4},{12,0},{16,28},{20,24},{24,20},{28,16},{1,13},{... | collective-permute-start | bytes 294920 | tf_op jit(solution)/shard_map/ppermute | solution.py:494
  180.9 14.3 %collective-permute-start.22 = (bf16[24,2048]{1,0:T(8,128)(2,1)}, bf16[24,2048]{1,0:T(8,128)(2,1)S(1)}, u32[]{:S(2)}, u32[]{:S(2)}) collective-permute-start(bf16[24,2048]{1,0:T(8,128)(2,1)} %get-tuple-element.62), channel_id=1, source_target_pairs={{0,16},{4,20},{8,24},{12,28},{16,0},{20,4},{24,8},{28,12},{1,17},{... | collective-permute-start | bytes 294920 | tf_op jit(solution)/shard_map/ppermute | solution.py:494
  183.2 12.0 %collective-permute-start.23 = (bf16[24,2048]{1,0:T(8,128)(2,1)}, bf16[24,2048]{1,0:T(8,128)(2,1)S(1)}, u32[]{:S(2)}, u32[]{:S(2)}) collective-permute-start(bf16[24,2048]{1,0:T(8,128)(2,1)} %get-tuple-element.63), channel_id=1, source_target_pairs={{0,20},{4,16},{8,28},{12,24},{16,4},{20,0},{24,12},{28,8},{1,21},{... | collective-permute-start | bytes 294920 | tf_op jit(solution)/shard_map/ppermute | solution.py:494
  183.9 11.4 %collective-permute-start.24 = (bf16[24,2048]{1,0:T(8,128)(2,1)S(1)}, bf16[24,2048]{1,0:T(8,128)(2,1)S(1)}, u32[]{:S(2)}, u32[]{:S(2)}) collective-permute-start(bf16[24,2048]{1,0:T(8,128)(2,1)S(1)} %copy-done.20), channel_id=1, source_target_pairs={{0,24},{4,28},{8,16},{12,20},{16,8},{20,12},{24,0},{28,4},{1,25},{... | collective-permute-start | bytes 294920 | tf_op jit(solution)/shard_map/ppermute | solution.py:494
  187.4 7.8 %collective-permute-start.25 = (bf16[24,2048]{1,0:T(8,128)(2,1)S(1)}, bf16[24,2048]{1,0:T(8,128)(2,1)S(1)}, u32[]{:S(2)}, u32[]{:S(2)}) collective-permute-start(bf16[24,2048]{1,0:T(8,128)(2,1)S(1)} %copy-done.19), channel_id=1, source_target_pairs={{0,28},{4,24},{8,20},{12,16},{16,12},{20,8},{24,4},{28,0},{1,29},{... | collective-permute-start | bytes 294920 | tf_op jit(solution)/shard_map/ppermute | solution.py:494
  (23 other events, 123.4 us)
